TPU v7x, 128 devices: a whole 4x4x4 slice. The times are simulated.
128 devices in a mesh: sp: 32 (over z, y, core), tp: 4 (over x).
Axes of the slice: x: 4, y: 4, z: 4, core: 2. Of those that a mesh axis runs over, the one named last changes fastest.
Arguments:
- resid: bfloat16 [8192, 2048], P(('sp', 'tp')), may hold values from -6 to 6
- query_a: bfloat16 [8192, 4, 128], P('sp', 'tp')
- key_a: bfloat16 [8192, 4, 128], P('sp', 'tp')
- value_a: bfloat16 [8192, 4, 128], P('sp', 'tp'), may hold values from -6 to 6
- query_b: bfloat16 [8192, 4, 256], P('sp', 'tp')
- key_b: bfloat16 [8192, 4, 256], P('sp', 'tp')
- value_b: bfloat16 [8192, 4, 128], P('sp', 'tp'), may hold values from -6 to 6
- lambda_a: float32 [4], P('tp'), may hold values from 0.3 to 0.8
- lambda_b: float32 [4], P('tp'), may hold values from 0.3 to 0.8
- head_gain: float32 [128], replicated, may hold values from 0.1 to 1.9
- out_weight: bfloat16 [1024, 2048], replicated, may hold values from -0.1875 to 0.1875
- norm_gain: float32 [2048], replicated, may hold values from 0.1 to 1.9
- expert_ids: int32 [8192, 4], P(('sp', 'tp')), may hold values from 0 to 127, all different within a row; in each aligned block of 64 rows (0 to 63, 64 to 127, ...) at most 4 rows name the same one
- expert_mix: float32 [8192, 4], P(('sp', 'tp')), may hold values from 0.2 to 1
- gate_experts: bfloat16 [128, 2048, 1024], P(('sp', 'tp')), may hold values from -0.125 to 0.125
- up_experts: bfloat16 [128, 2048, 1024], P(('sp', 'tp')), may hold values from -0.125 to 0.125
- down_experts: bfloat16 [128, 1024, 2048], P(('sp', 'tp')), may hold values from -0.1875 to 0.1875
- shared_gate: bfloat16 [2048, 512], replicated, may hold values from -0.125 to 0.125
- shared_up: bfloat16 [2048, 512], replicated, may hold values from -0.125 to 0.125
- shared_down: bfloat16 [512, 2048], replicated, may hold values from -0.25 to 0.25
Outputs:
- layer_out: bfloat16 [8192, 2048], P(('sp', 'tp'))
Inputs may be any that keep to these rules, and one draw needn't show every extreme that they name: `expert_ids`: in each aligned block of 64 rows (the rows of one device) no expert is named more than 4 times, a bound that some block reaches.
All inputs are finite; a program needn't handle non-finite values.
Results may differ from a plain program's by a relative error of at most 0.017.
Values may be sent and summed in bfloat16 or wider, within the bound.
A program may use at most 128 MiB of HBM per device.

v0:
```python
import math

import jax
import jax.numpy as jnp
from jax import lax
from jax.sharding import PartitionSpec as P

NEG_FILL = -1e30
EPSILON = 1e-05
HEAD_SCALE = 0.8
KEY_SPAN = 2048


def sent_together(arrays, axis, dim, along):
    widths = [a.shape[along] for a in arrays]
    both = jnp.concatenate(arrays, axis=along)
    whole = lax.all_gather(both, axis, axis=dim, tiled=True)
    return tuple(jnp.split(whole, [sum(widths[:k]) for k in range(1, len(widths))], axis=along))


def side_by_side(arrays, axis, split_dim, concat_dim, along):
    both = jnp.concatenate(arrays, axis=along)
    whole, at, outs = (
        lax.all_to_all(both, axis, split_axis=split_dim, concat_axis=concat_dim, tiled=True),
        0,
        [],
    )
    for a in arrays:
        outs.append(lax.slice_in_dim(whole, at, at + a.shape[along], axis=along))
        at += a.shape[along]
    return tuple(outs)


def split_up(value, dim, devices):
    lengths = value.shape
    tiles = value.reshape(*lengths[:dim], devices, lengths[dim] // devices, *lengths[dim + 1 :])
    return jnp.moveaxis(tiles, dim, 0)


def laid_out(tiles, dim):
    tiles = jnp.moveaxis(tiles, 0, dim)
    lengths = tiles.shape
    return tiles.reshape(*lengths[:dim], lengths[dim] * lengths[dim + 1], *lengths[dim + 2 :])


def joined_exchange(value, axis, axes, splits, concats):
    sizes = [lax.axis_size(a) for a in axes]
    tiles = split_up(value, splits[0], sizes[0])
    tiles = jnp.moveaxis(split_up(tiles, splits[1] + 1, sizes[1]), 0, 1)
    inside = tiles.shape[2:]
    tiles = tiles.reshape(-1, *inside)
    tiles = lax.all_to_all(tiles, axis, split_axis=0, concat_axis=0, tiled=True)
    tiles = laid_out(tiles.reshape(*sizes, *inside), concats[0] + 1)
    return laid_out(tiles, concats[1])


def swiglu_rows(row_set, w_gate, w_up, w_down):
    gate_val = jnp.dot(row_set, w_gate, preferred_element_type=jnp.float32)
    up_val = jnp.dot(row_set, w_up, preferred_element_type=jnp.float32)
    hidden = (jax.nn.silu(gate_val) * up_val).astype(jnp.bfloat16)
    return jnp.dot(hidden, w_down, preferred_element_type=jnp.float32)


def online_update(state, query_map, key_map, value_block, causal, scaling):
    row_top, denoms, numerator = state
    scores = (
        jnp.einsum("qhd,khd->hqk", query_map, key_map, preferred_element_type=jnp.float32) * scaling
    )
    scores = jnp.where(causal, scores, NEG_FILL)
    new_top = jnp.maximum(row_top, jnp.max(scores, axis=2))
    exponent = jnp.where(causal, jnp.exp(scores - new_top[:, :, None]), 0.0)
    shrink = jnp.exp(row_top - new_top)
    denoms = denoms * shrink + jnp.sum(exponent, axis=2)
    numerator = numerator * jnp.transpose(shrink)[:, :, None] + jnp.einsum(
        "hqk,khe->qhe",
        exponent.astype(jnp.bfloat16),
        value_block,
        preferred_element_type=jnp.float32,
    )
    return (new_top, denoms, numerator)


def group_update(states, queries, key_block, value_block, causal):
    map_width = queries.shape[2] // 2
    scaling = map_width ** (-0.5)
    first_state = online_update(
        states[0],
        queries[:, :, :map_width],
        key_block[:, :, :map_width],
        value_block,
        causal,
        scaling,
    )
    second_state = online_update(
        states[1],
        queries[:, :, map_width:],
        key_block[:, :, map_width:],
        value_block,
        causal,
        scaling,
    )
    return (first_state, second_state)


def empty_state(query_rows, head_count, value_width):
    single = (
        jnp.full((head_count, query_rows), NEG_FILL, jnp.float32),
        jnp.zeros((head_count, query_rows), jnp.float32),
        jnp.zeros((query_rows, head_count, value_width), jnp.float32),
    )
    return (single, single)


def finish_group(states, lambdas, head_gain):
    first_out = states[0][2] / jnp.transpose(states[0][1])[:, :, None]
    second_out = states[1][2] / jnp.transpose(states[1][1])[:, :, None]
    differ = first_out - lambdas[None, :, None] * second_out
    scale_rms = lax.rsqrt(jnp.mean(differ * differ, axis=2, keepdims=True) + EPSILON)
    return (differ * scale_rms * head_gain[None, None, :] * HEAD_SCALE).astype(jnp.bfloat16)


def per_device(
    resid,
    query_a,
    key_a,
    value_a,
    query_b,
    key_b,
    value_b,
    lambda_a,
    lambda_b,
    head_gain,
    out_weight,
    norm_gain,
    expert_ids,
    expert_mix,
    gate_experts,
    up_experts,
    down_experts,
    shared_gate,
    shared_up,
    shared_down,
):
    query_rows = query_a.shape[0]
    value_width = value_a.shape[2]
    query_pos = lax.axis_index("sp") * query_rows + jnp.arange(query_rows, dtype=jnp.int32)
    start_state = (
        empty_state(query_rows, query_a.shape[1], value_width),
        empty_state(query_rows, query_b.shape[1], value_width),
    )
    key_piece_a, value_piece_a, key_piece_b, value_piece_b = sent_together(
        (key_a, value_a, key_b, value_b), "sp", 0, 2
    )
    piece_rows = key_piece_a.shape[0]
    step_rows = math.gcd(piece_rows, KEY_SPAN)

    def one_step(step_index, inner_state):
        begin_row = step_index * step_rows
        key_pos = begin_row + jnp.arange(step_rows, dtype=jnp.int32)
        causal = (key_pos[None, :] <= query_pos[:, None])[None]
        part_a = group_update(
            inner_state[0],
            query_a,
            lax.dynamic_slice_in_dim(key_piece_a, begin_row, step_rows, 0),
            lax.dynamic_slice_in_dim(value_piece_a, begin_row, step_rows, 0),
            causal,
        )
        part_b = group_update(
            inner_state[1],
            query_b,
            lax.dynamic_slice_in_dim(key_piece_b, begin_row, step_rows, 0),
            lax.dynamic_slice_in_dim(value_piece_b, begin_row, step_rows, 0),
            causal,
        )
        return (part_a, part_b)

    state_a, state_b = lax.fori_loop(0, piece_rows // step_rows, one_step, start_state)
    heads_a = finish_group(state_a, lambda_a, head_gain)
    heads_b = finish_group(state_b, lambda_b, head_gain)
    tok_dev = resid.shape[0]
    back_a, back_b = side_by_side((heads_a, heads_b), "tp", 0, 1, 2)
    joined = jnp.concatenate([back_a.reshape(tok_dev, -1), back_b.reshape(tok_dev, -1)], axis=1)
    project = jnp.dot(joined, out_weight, preferred_element_type=jnp.float32)
    middle = (resid.astype(jnp.float32) + project).astype(jnp.bfloat16)
    middle_f = middle.astype(jnp.float32)
    normed = (
        middle_f
        * lax.rsqrt(jnp.mean(middle_f * middle_f, axis=1, keepdims=True) + EPSILON)
        * norm_gain[None, :]
    ).astype(jnp.bfloat16)
    shared = swiglu_rows(normed, shared_gate, shared_up, shared_down)
    top_count = expert_ids.shape[1]
    model_width = normed.shape[1]
    sp_count = lax.axis_size("sp")
    tp_count = lax.axis_size("tp")
    expert_total = sp_count * tp_count
    pair_count = tok_dev * top_count
    capacity = max(2, 2 * pair_count // expert_total)
    flat_ids = expert_ids.reshape(-1)
    one_hot = (flat_ids[:, None] == jnp.arange(expert_total, dtype=jnp.int32)[None, :]).astype(
        jnp.int32
    )
    pair_rank = jnp.sum((jnp.cumsum(one_hot, axis=0) - one_hot) * one_hot, axis=1)
    pair_token = jnp.arange(pair_count, dtype=jnp.int32) // top_count
    send_rows = (
        jnp.zeros((expert_total, capacity, model_width), jnp.bfloat16)
        .at[flat_ids, pair_rank]
        .set(normed[pair_token])
    )
    grid_rows = send_rows.reshape(sp_count, tp_count, capacity, model_width)
    arrived = joined_exchange(grid_rows, ("sp", "tp"), ("sp", "tp"), (0, 1), (0, 1))
    arrived_shape = arrived.shape
    flat_rows = arrived.reshape(-1, arrived_shape[-1])
    result = swiglu_rows(flat_rows, gate_experts[0], up_experts[0], down_experts[0]).astype(
        jnp.bfloat16
    )
    finished = result.reshape(arrived_shape)
    returned = joined_exchange(finished, ("sp", "tp"), ("sp", "tp"), (0, 1), (0, 1))
    returned = returned.reshape(expert_total, capacity, model_width)
    chosen = returned[flat_ids, pair_rank].reshape(tok_dev, top_count, model_width)
    routed = jnp.sum(chosen.astype(jnp.float32) * expert_mix[:, :, None], axis=1)
    return (middle_f + shared + routed).astype(jnp.bfloat16)


def solution(mesh):
    in_specs = (
        P(("sp", "tp"), None),
        P("sp", "tp", None),
        P("sp", "tp", None),
        P("sp", "tp", None),
        P("sp", "tp", None),
        P("sp", "tp", None),
        P("sp", "tp", None),
        P("tp"),
        P("tp"),
        P(),
        P(),
        P(),
        P(("sp", "tp"), None),
        P(("sp", "tp"), None),
        P(("sp", "tp"), None, None),
        P(("sp", "tp"), None, None),
        P(("sp", "tp"), None, None),
        P(),
        P(),
        P(),
    )
    out_specs = P(("sp", "tp"), None)
    return jax.shard_map(
        per_device, mesh=mesh, in_specs=in_specs, out_specs=out_specs, check_vma=False
    )
```

profile of v0, /device:TPU:1, one launch (start us, length us, event | category | flops | bytes accessed | tf_op | source)
XLA Modules:
  0.0 339.5 jit_solution(6949702209437648387)
XLA Ops:
  6.5 1.9 pad_maximum_fusion
  8.6 0.8 copy.67
  11.6 59.4 %all-gather.2.cloned.1.call-done = bf16[8192,1,640]{2,0,1:T(8,128)(2,1)} async-done(((bf16[256,1,640]{2,0,1:T(8,128)(2,1)}), bf16[8192,1,640]{2,0,1:T(8,128)(2,1)}) %all-gather.2.cloned.1.call-update) | async-done | bytes 10485776 | tf_op jit(solution)/shard_map/all_gather | solution.py:17
  71.0 5.7 %fusion.115 = (bf16[8192,1,128]{2,0,1:T(8,128)(2,1)}, bf16[8192,1,128]{2,0,1:T(8,128)(2,1)}, bf16[8192,1,128]{2,0,1:T(8,128)(2,1)}) fusion(bf16[8192,1,640]{2,0,1:T(8,128)(2,1)} %all-gather.2.cloned.1.call-done), kind=kLoop, calls=%fused_computation.182 | loop fusion | bytes 12582912 | tf_op jit(solution)/shard_map/split | solution.py:18
  76.7 4.6 %split.18 = bf16[8192,1,256]{2,0,1:T(8,128)(2,1)} slice(bf16[8192,1,640]{2,0,1:T(8,128)(2,1)} %all-gather.2.cloned.1.call-done), slice={[0:8192], [0:1], [256:512]} | slice | bytes 8388608 | tf_op jit(solution)/shard_map/split | solution.py:18
  81.3 74.1 %while.36 = (s32[]{:T(128)}, f32[1,256]{1,0:T(1,128)S(1)}, f32[1,256]{1,0:T(1,128)S(1)}, f32[256,1,128]{0,2,1:T(8,128)S(1)}, f32[1,256]{1,0:T(1,128)S(1)}, /*ind...) while((s32[]{:T(128)}, f32[1,256]{1,0:T(1,128)S(1)}, ...), condition=%wide.region_9.10_spmd.clone, body=%wide.region_0.9_spmd.clone.sunk | while | flops 963517696 | bytes 72772088 | solution.py:177
  81.3 3.0 fusion.162
  84.3 2.9 fusion.160
  87.2 2.9 fusion.156
  90.1 1.8 fusion.158
  92.0 3.2 fusion.164
  95.3 0.7 fusion.170
  96.0 0.9 copy-done.3
  97.7 0.7 fusion.167
  98.4 0.7 copy-done.2
  99.1 0.6 fusion.166
  99.8 3.0 fusion.162
  102.8 2.9 fusion.160
  105.7 2.9 fusion.156
  108.6 1.8 fusion.158
  110.5 3.2 fusion.164
  113.8 0.7 fusion.170
  114.5 0.9 copy-done.3
  116.2 0.7 fusion.167
  116.9 0.7 copy-done.2
  118.4 3.0 fusion.162
  121.4 2.9 fusion.160
  124.2 2.9 fusion.156
  127.2 1.8 fusion.158
  129.1 3.2 fusion.164
  132.3 0.7 fusion.170
  133.0 0.9 copy-done.3
  134.8 0.7 fusion.167
  135.4 0.7 copy-done.2
  136.9 3.0 fusion.162
  139.9 2.9 fusion.160
  142.8 2.9 fusion.156
  145.7 1.8 fusion.158
  147.6 3.2 fusion.164
  150.9 0.7 fusion.170
  151.6 0.9 copy-done.3
  153.3 0.7 fusion.167
  154.0 0.7 copy-done.2
  156.9 0.7 reduce.34
  157.5 0.7 reshape.394
  158.2 4.0 %all-to-all-start = ((bf16[4,2,8192]{2,1,0:T(2,128)(2,1)}), bf16[4,2,8192]{2,1,0:T(2,128)(2,1)S(1)}, u32[]{:S(2)}, u32[]{:S(2)}) async-start(bf16[4,2,8192]{2,1,0:T(2,128)(2,1)} %reshape.394), calls=%async_computation | async-start | bytes 262144 | tf_op jit(solution)/shard_map/all_to_all | solution.py:24
  162.2 4.8 %all-to-all-done = bf16[4,2,8192]{2,1,0:T(2,128)(2,1)S(1)} async-done(((bf16[4,2,8192]{2,1,0:T(2,128)(2,1)}), bf16[4,2,8192]{2,1,0:T(2,128)(2,1)S(1)}, u32[]{:S(2)}, u32[]{:S(2)}) %all-to-all-start) | async-done | bytes 131104 | tf_op jit(solution)/shard_map/all_to_all | solution.py:24
  167.3 3.2 multiply_reduce_fusion.1
  170.6 2.3 gather_fusion
  172.9 2.4 broadcast_in_dim.56
  175.3 44.6 %scatter_fusion = bf16[128,4,2048]{2,1,0:T(4,128)(2,1)} fusion(bf16[128,4,2048]{2,1,0:T(4,128)(2,1)} %broadcast_in_dim.56, s32[256]{0:T(256)S(1)} %bitcast.257, bf16[256,2048]{1,0:T(8,128)(2,1)} %gather_fusion), kind=kCustom, calls=%fused_computation.2 | custom fusion | bytes 3147776 | tf_op jit(solution)/shard_map/scatter | solution.py:208
  219.9 37.8 %all_to_all.28 = bf16[128,1,1,4,2048]{4,3,2,1,0:T(4,128)(2,1)} all-to-all(bf16[128,1,1,4,2048]{4,3,2,1,0:T(4,128)(2,1)} %bitcast.255), channel_id=1, replica_groups=mesh['sp'=32,'tp'=4] {'sp','tp'}, dimensions={0} | all-to-all | bytes 4194304 | tf_op jit(solution)/shard_map/all_to_all | solution.py:52
  257.7 4.0 %reshape_reshape.6 = bf16[512,2048]{1,0:T(8,128)(2,1)} reshape(bf16[32,4,1,4,2048]{4,3,1,0,2:T(4,128)(2,1)} %bitcast.259) | data formatting | bytes 4194304 | tf_op jit(solution)/shard_map/reshape;reshape | solution.py:213
  261.6 6.5 %fusion.78 = f32[512,1024]{1,0:T(8,128)} fusion(bf16[512,2048]{1,0:T(8,128)(2,1)} %reshape_reshape.6, bf16[1,2048,1024]{2,1,0:T(8,128)(2,1)} %param.36), kind=kOutput, calls=%fused_computation.114 | convolution fusion | flops 2147483648 | bytes 8388608 | tf_op jit(solution)/shard_map/dot_general | solution.py:58
  268.1 10.5 %fusion.80 = bf16[512,2048]{1,0:T(8,128)(2,1)} fusion(bf16[1,1024,2048]{2,1,0:T(8,128)(2,1)} %param.38, f32[512,1024]{1,0:T(8,128)} %fusion.78, bf16[512,2048]{1,0:T(8,128)(2,1)} %reshape_reshape.6, bf16[1,2048,1024]{2,1,0:T(8,128)(2,1)} %param.37), kind=kOutput, calls=%fused_computation.116 | convolution fusion | flops 4299161600 | bytes 14680064 | tf_op jit(solution)/shard_map/dot_general | solution.py:61
  278.7 4.1 %reshape_transpose_transpose_reshape_reshape_reshape.7 = bf16[128,1,1,4,2048]{4,3,0,2,1:T(4,128)(2,1)} reshape(bf16[512,2048]{1,0:T(8,128)(2,1)} %fusion.80) | data formatting | bytes 4194304 | tf_op jit(solution)/shard_map/reshape;transpose;transpose;reshape;reshape;reshape | solution.py:51
  282.8 5.0 %all-to-all-start.2 = ((bf16[128,1,1,4,2048]{4,3,2,1,0:T(4,128)(2,1)}), bf16[128,1,1,4,2048]{4,3,2,1,0:T(4,128)(2,1)}, u32[]{:S(2)}, u32[]{:S(2)}) async-start(bf16[128,1,1,4,2048]{4,3,2,1,0:T(4,128)(2,1)} %bitcast.258), calls=%async_computation.2 | async-start | bytes 4194304 | tf_op jit(solution)/shard_map/all_to_all | solution.py:52
  287.8 0.7 copy.73
  288.5 2.1 fusion.116
  290.5 27.8 %all-to-all-done.2 = bf16[128,1,1,4,2048]{4,3,2,1,0:T(4,128)(2,1)} async-done(((bf16[128,1,1,4,2048]{4,3,2,1,0:T(4,128)(2,1)}), bf16[128,1,1,4,2048]{4,3,2,1,0:T(4,128)(2,1)}, u32[]{:S(2)}, u32[]{:S(2)}) %all-to-all-start.2) | async-done | bytes 2097184 | tf_op jit(solution)/shard_map/all_to_all | solution.py:52
  318.3 5.2 %gather_fusion.1 = bf16[256,2048]{1,0:T(8,128)(2,1)} fusion(bf16[128,4,2048]{2,1,0:T(4,128)(2,1)} %bitcast.28, s32[256]{0:T(256)S(1)} %bitcast.256), kind=kCustom, calls=%fused_computation.1 | custom fusion | bytes 2099200 | tf_op jit(solution)/shard_map/gather | solution.py:220
  323.5 2.7 reshape.363
  326.2 3.2 multiply_reduce_fusion
  329.4 3.2 fusion.84
  (147 shorter events, 8.4 us)
Async XLA Ops:
  6.5 322.9 %copy-start = (bf16[512,2048]{1,0:T(8,128)(2,1)S(1)}, bf16[512,2048]{1,0:T(8,128)(2,1)}, u32[]{:S(2)}) copy-start(bf16[512,2048]{1,0:T(8,128)(2,1)} %param.41) | copy-start | bytes 6291460
  6.5 64.5 %all-gather.2.cloned.1.call-start = ((), (), s32[]{:S(2)}) async-start(), calls=%async_computation.3 | async-start | bytes 10813440 | tf_op jit(solution)/shard_map/all_gather | solution.py:17
  76.7 4.6 %copy-start.10 = (bf16[256,1,256]{2,0,1:T(8,128)(2,1)S(1)}, bf16[256,1,256]{2,0,1:T(8,128)(2,1)}, u32[]{:S(2)}) copy-start(bf16[256,1,256]{2,0,1:T(8,128)(2,1)} %param.26) | copy-start | bytes 393220
  76.7 4.6 %copy-start.11 = (bf16[256,1,128]{2,0,1:T(8,128)(2,1)S(1)}, bf16[256,1,128]{2,0,1:T(8,128)(2,1)}, u32[]{:S(2)}) copy-start(bf16[256,1,128]{2,0,1:T(8,128)(2,1)} %param.23) | copy-start | bytes 196612
  81.3 74.9 %copy-start.9 = (f32[128]{0:T(128)S(1)}, f32[128]{0:T(128)}, u32[]{:S(2)}) copy-start(f32[128]{0:T(128)} %param.31) | copy-start | bytes 1540
  90.1 1.9 copy-start.1
  92.0 3.3 copy-start.4
  95.2 1.6 copy-start.3
  96.0 1.7 copy-start.5
  97.5 1.7 copy-start.2
  108.6 1.9 copy-start.1
  110.5 3.3 copy-start.4
  113.8 1.6 copy-start.3
  114.5 1.7 copy-start.5
  116.0 1.6 copy-start.2
  127.2 1.9 copy-start.1
  129.0 3.3 copy-start.4
  132.3 1.6 copy-start.3
  133.0 1.7 copy-start.5
  134.5 1.7 copy-start.2
  145.7 1.9 copy-start.1
  147.6 3.3 copy-start.4
  150.8 1.6 copy-start.3
  151.5 1.7 copy-start.5
  153.1 1.6 copy-start.2
  155.6 11.6 %copy-start.6 = (bf16[64,2048]{1,0:T(8,128)(2,1)S(1)}, bf16[64,2048]{1,0:T(8,128)(2,1)}, u32[]{:S(2)}) copy-start(bf16[64,2048]{1,0:T(8,128)(2,1)} %param.22) | copy-start | bytes 786436
  158.2 8.8 %all-to-all-start = ((bf16[4,2,8192]{2,1,0:T(2,128)(2,1)}), bf16[4,2,8192]{2,1,0:T(2,128)(2,1)S(1)}, u32[]{:S(2)}, u32[]{:S(2)}) async-start(bf16[4,2,8192]{2,1,0:T(2,128)(2,1)} %reshape.394), calls=%async_computation | async-start | bytes 262144 | tf_op jit(solution)/shard_map/all_to_all | solution.py:24
  167.2 3.2 copy-start.7
  282.8 5.0 %copy-start.8 = (f32[64,4]{0,1:T(4,128)S(1)}, f32[64,4]{0,1:T(4,128)}, u32[]{:S(2)}) copy-start(f32[64,4]{0,1:T(4,128)} %param.35) | copy-start | bytes 3076
  282.8 35.5 %all-to-all-start.2 = ((bf16[128,1,1,4,2048]{4,3,2,1,0:T(4,128)(2,1)}), bf16[128,1,1,4,2048]{4,3,2,1,0:T(4,128)(2,1)}, u32[]{:S(2)}, u32[]{:S(2)}) async-start(bf16[128,1,1,4,2048]{4,3,2,1,0:T(4,128)(2,1)} %bitcast.258), calls=%async_computation.2 | async-start | bytes 4194304 | tf_op jit(solution)/shard_map/all_to_all | solution.py:52
Sparse Core Ops, SparseCore 0:
  9.6 61.3 all-gather.1
where the time goes:
time: 342 us; the launch traced here: 340 us
  waiting for transfers between devices  92 us (27%)
  local copies, waits for them, and re-layouts  86.5 us (25%)
  matrix products  78.4 us (23%)
  blocking collectives  37.8 us (11%)
  other arithmetic  20.1 us (6%)
  between operations  15.1 us (4%)
  starting transfers between devices  8.93 us (3%)
    all_gather x1, waiting for transfers between devices, sent_together(): whole = lax.all_gather(both, axis, axis=dim, tiled=True)  59.4 us
    scatter x1, local copies, waits for them, and re-layouts, per_device(): send_rows = jnp.zeros((expert_total, capacity, model_width), jnp.bfloat16...  44.6 us
    dot_general x16, matrix products, online_update(): jnp.einsum('qhd,khd->hqk', query_map, key_map, preferred_element_type=jnp...  42.4 us
    all_to_all x1, blocking collectives, joined_exchange(): tiles = lax.all_to_all(tiles, axis, split_axis=0, concat_axis=0, tiled=True)  37.8 us
    all_to_all x1, waiting for transfers between devices, joined_exchange(): tiles = lax.all_to_all(tiles, axis, split_axis=0, concat_axis=0, tiled=True)  27.8 us
    dot_general x2, matrix products, swiglu_rows(): return jnp.dot(hidden, w_down, preferred_element_type=jnp.float32)  13.8 us
    reduce_sum x4, other arithmetic, online_update(): denoms = denoms * shrink + jnp.sum(exponent, axis=2)  12.9 us
    dot_general x16, matrix products, online_update(): jnp.einsum('hqk,khe->qhe', exponent.astype(jnp.bfloat16), value_block, pr...  10.5 us
  transfers between devices with their start and end apart: 3, of which 3 were waited for; matrix products, arithmetic and copies ran while one was open for 1% of the time, Pallas kernels for 0%

commit v1 on v0

v1 whole, which is shorter than its diff:
```python
import functools
import math

import jax
import jax.numpy as jnp
from jax import lax
from jax.experimental import pallas as pl
from jax.experimental.pallas import tpu as pltpu
from jax.sharding import PartitionSpec as P

EPSILON = 1e-05
HEAD_SCALE = 0.8
LOG2E = 1.4426950408889634
NEG = -1e30
BF16 = jnp.bfloat16
F32 = jnp.float32


def dot_nt(a, b):
    return lax.dot_general(a, b, (((1,), (1,)), ((), ())), preferred_element_type=F32)


def attention_kernel(q_ref, kv_ref, lam_ref, gain_ref, out_ref, acc, top):
    me = lax.axis_index("sp")
    chip = me // 2
    rows = q_ref.shape[0]
    ones = jnp.ones((8, 2 * rows), BF16)
    scale_a = LOG2E * 64**-0.5
    scale_b = LOG2E * 128**-0.5

    def chunk(c, masked, first):
        piece = [kv_ref.at[2 * c], kv_ref.at[2 * c + 1]]
        if masked:
            key_pos = lax.broadcasted_iota(jnp.int32, (2 * rows, rows), 0)
            query_pos = lax.broadcasted_iota(jnp.int32, (2 * rows, rows), 1) + (me % 2) * rows
            keep = key_pos <= query_pos
        for head in range(2):
            vt = jnp.concatenate(
                [p[head * 128 : head * 128 + 128, 384:640] for p in piece], axis=1
            )
            vt = jnp.concatenate([vt, ones], axis=0)
            for m in range(2):
                h = head * 2 + m
                lo = [0, 0, 128, 256][h]
                keys = jnp.concatenate([p[:, lo : lo + 128] for p in piece], axis=0)
                s = dot_nt(keys, q_ref[:, h * 128 : h * 128 + 128])
                s = s * (scale_a if head == 0 else scale_b)
                if masked:
                    s = jnp.where(keep, s, NEG)
                best = jnp.max(s, axis=0, keepdims=True)
                if not first:
                    old = top[h : h + 1, :]
                    best = jnp.maximum(best, old)
                p = jnp.exp2(s - best).astype(BF16)
                add = jnp.dot(vt, p, preferred_element_type=F32)
                if first:
                    acc[h] = add
                else:
                    acc[h] = acc[h] * jnp.exp2(old - best) + add
                top[h : h + 1, :] = best

    chunk(chip, True, True)

    def body(c, carry):
        chunk(c, False, False)
        return carry

    lax.fori_loop(0, chip, body, 0)
    for head in range(2):
        first = acc[2 * head]
        second = acc[2 * head + 1]
        one = first[0:128] / first[128:129]
        two = second[0:128] / second[128:129]
        differ = one - lam_ref[head] * two
        scale = lax.rsqrt(jnp.mean(differ * differ, axis=0, keepdims=True) + EPSILON)
        heads = differ * scale
        out_ref[:, head * 128 : head * 128 + 128] = (
            heads.T * gain_ref[...] * HEAD_SCALE
        ).astype(BF16)


def attention(q, kv, lam, gain):
    rows = q.shape[0]
    return pl.pallas_call(
        attention_kernel,
        out_shape=jax.ShapeDtypeStruct((rows, 256), BF16),
        in_specs=[
            pl.BlockSpec(memory_space=pltpu.VMEM),
            pl.BlockSpec(memory_space=pltpu.VMEM),
            pl.BlockSpec(memory_space=pltpu.SMEM),
            pl.BlockSpec(memory_space=pltpu.VMEM),
        ],
        out_specs=pl.BlockSpec(memory_space=pltpu.VMEM),
        scratch_shapes=[
            pltpu.VMEM((4, 136, rows), F32),
            pltpu.VMEM((8, rows), F32),
        ],
        compiler_params=pltpu.CompilerParams(vmem_limit_bytes=48 * 1024 * 1024),
    )(q, kv, lam, gain)


def swiglu_rows(row_set, w_gate, w_up, w_down):
    gate_val = jnp.dot(row_set, w_gate, preferred_element_type=F32)
    up_val = jnp.dot(row_set, w_up, preferred_element_type=F32)
    hidden = (jax.nn.silu(gate_val) * up_val).astype(BF16)
    return jnp.dot(hidden, w_down, preferred_element_type=F32)


def slot_matrices(expert_ids, expert_mix, experts, capacity):
    tokens, top_count = expert_ids.shape
    named = jnp.sum(
        (expert_ids[:, :, None] == jnp.arange(experts, dtype=jnp.int32)).astype(F32), axis=1
    )
    mix = jnp.sum(
        jnp.where(
            expert_ids[:, :, None] == jnp.arange(experts, dtype=jnp.int32),
            expert_mix[:, :, None],
            0.0,
        ),
        axis=1,
    )
    before = jnp.tril(jnp.ones((tokens, tokens), F32), -1)
    rank = jnp.dot(before, named, preferred_element_type=F32)
    slot = jnp.arange(capacity, dtype=F32)
    hit = (rank[:, :, None] == slot) & (named[:, :, None] > 0)
    fill = hit.astype(BF16).reshape(tokens, experts * capacity)
    weight = jnp.where(hit, mix[:, :, None], 0.0).reshape(tokens, experts * capacity)
    return fill, weight


def per_device(
    resid,
    query_a,
    key_a,
    value_a,
    query_b,
    key_b,
    value_b,
    lambda_a,
    lambda_b,
    head_gain,
    out_weight,
    norm_gain,
    expert_ids,
    expert_mix,
    gate_experts,
    up_experts,
    down_experts,
    shared_gate,
    shared_up,
    shared_down,
):
    rows = query_a.shape[0]
    sp_count = lax.axis_size("sp")
    tp_count = lax.axis_size("tp")
    experts = sp_count * tp_count
    tok_dev, width = resid.shape
    capacity = 4
    qa = query_a[:, 0]
    zero = jnp.zeros((rows, 64), BF16)
    q = jnp.concatenate([qa[:, :64], zero, zero, qa[:, 64:], query_b[:, 0]], axis=1)
    piece = jnp.concatenate(
        [
            key_a[:, 0],
            key_b[:, 0],
            jnp.concatenate([value_a[:, 0].T, value_b[:, 0].T], axis=0),
        ],
        axis=1,
    )
    kv = lax.all_gather(piece, "sp", axis=0, tiled=False)
    lam = jnp.concatenate([lambda_a, lambda_b])
    heads = attention(q, kv, lam, head_gain[None, :])
    back = lax.all_to_all(
        heads.reshape(tp_count, tok_dev, 256), "tp", split_axis=0, concat_axis=0, tiled=True
    )
    joined = jnp.concatenate(
        [back[:, :, :128].transpose(1, 0, 2).reshape(tok_dev, -1),
         back[:, :, 128:].transpose(1, 0, 2).reshape(tok_dev, -1)], axis=1)
    project = jnp.dot(joined, out_weight, preferred_element_type=F32)
    middle = (resid.astype(F32) + project).astype(BF16)
    middle_f = middle.astype(F32)
    normed = (
        middle_f
        * lax.rsqrt(jnp.mean(middle_f * middle_f, axis=1, keepdims=True) + EPSILON)
        * norm_gain[None, :]
    ).astype(BF16)
    shared = swiglu_rows(normed, shared_gate, shared_up, shared_down)
    fill, weight = slot_matrices(expert_ids, expert_mix, experts, capacity)
    send = jnp.dot(fill.T, normed, preferred_element_type=F32).astype(BF16)
    arrived = lax.all_to_all(send, ("sp", "tp"), split_axis=0, concat_axis=0, tiled=True)
    result = swiglu_rows(arrived, gate_experts[0], up_experts[0], down_experts[0]).astype(BF16)
    returned = lax.all_to_all(result, ("sp", "tp"), split_axis=0, concat_axis=0, tiled=True)
    high = weight.astype(BF16)
    low = (weight - high.astype(F32)).astype(BF16)
    routed = jnp.dot(high, returned, preferred_element_type=F32) + jnp.dot(
        low, returned, preferred_element_type=F32
    )
    return (middle_f + shared + routed).astype(BF16)


def solution(mesh):
    in_specs = (
        P(("sp", "tp"), None),
        P("sp", "tp", None),
        P("sp", "tp", None),
        P("sp", "tp", None),
        P("sp", "tp", None),
        P("sp", "tp", None),
        P("sp", "tp", None),
        P("tp"),
        P("tp"),
        P(),
        P(),
        P(),
        P(("sp", "tp"), None),
        P(("sp", "tp"), None),
        P(("sp", "tp"), None, None),
        P(("sp", "tp"), None, None),
        P(("sp", "tp"), None, None),
        P(),
        P(),
        P(),
    )
    return jax.shard_map(
        per_device,
        mesh=mesh,
        in_specs=in_specs,
        out_specs=P(("sp", "tp"), None),
        check_vma=False,
    )
```

time: 342 us -> 261 us (0.76)
  local copies, waits for them, and re-layouts: 86.5 us -> 30.2 us
  matrix products: 78.4 us -> 35.8 us
  blocking collectives: 37.8 us -> 63 us
  other arithmetic: 20.1 us -> 3.58 us
  Pallas kernels: 0 us -> 6.71 us
  waiting for transfers between devices: 92 us -> 96.2 us
    scatter x1 -> x0, local copies, waits for them, and re-layouts: 44.6 us -> none  [per_device(): send_rows = jnp.zeros((expert_total, capacity, model_width), jnp.bfloat16...]
    dot_general x37 -> x9, matrix products: 78.4 us -> 35.8 us  [the longest x2 13.8 us: swiglu_rows(): return jnp.dot(hidden, w_down, preferred_element_type=F32)]
    all_to_all x1, blocking collectives: 37.8 us -> 63 us  [per_device(): lax.all_to_all(send, ('sp', 'tp'), split_axis=0, concat_axis=0, tiled=True)]
    reduce_sum x7 -> x1, other arithmetic: 16.6 us -> 0.83 us  [slot_matrices(): jnp.sum(jnp.where(expert_ids[:, :, None] == jnp.arange(experts, dtype=jnp...]
    all_gather x0 -> x1, local copies, waits for them, and re-layouts: none -> 14.4 us  [per_device(): kv = lax.all_gather(piece, 'sp', axis=0, tiled=False)]
    all_to_all x0 -> x3, local copies, waits for them, and re-layouts: none -> 12.1 us  [the longest x2 8.04 us: per_device(): lax.all_to_all(send, ('sp', 'tp'), split_axis=0, concat_axis=0, tiled=True)]
    split x2 -> x0, local copies, waits for them, and re-layouts: 10.2 us -> none  [sent_together(): jnp.split(whole, [sum(widths[:k]) for k in range(1, len(widths))], axis=a...]
    another operation x5 -> x0, local copies, waits for them, and re-layouts: 8.09 us -> none  [the longest x1 4.11 us: joined_exchange(): tiles = tiles.reshape(-1, *inside)]
  transfers between devices with their start and end apart: 3 -> 3, of which waited for: 3 -> 3; matrix products, arithmetic and copies ran while one was open for 1% -> 2% of each run, Pallas kernels for 0% -> 0%
where the time goes in v1:
time: 261 us; the launch traced here: 259 us
  waiting for transfers between devices  96.2 us (37%)
  blocking collectives  63 us (24%)
  matrix products  35.8 us (14%)
  local copies, waits for them, and re-layouts  30.2 us (12%)
  between operations  14.9 us (6%)
  starting transfers between devices  8.86 us (3%)
  Pallas kernels  6.71 us (3%)
  other arithmetic  3.58 us (1%)
    all_gather x1, waiting for transfers between devices, per_device(): kv = lax.all_gather(piece, 'sp', axis=0, tiled=False)  63.4 us
    all_to_all x1, blocking collectives, per_device(): lax.all_to_all(send, ('sp', 'tp'), split_axis=0, concat_axis=0, tiled=True)  63 us
    all_to_all x1, waiting for transfers between devices, per_device(): lax.all_to_all(result, ('sp', 'tp'), split_axis=0, concat_axis=0, tiled=T...  28.4 us
    all_gather x1, local copies, waits for them, and re-layouts, per_device(): kv = lax.all_gather(piece, 'sp', axis=0, tiled=False)  14.4 us
    dot_general x2, matrix products, swiglu_rows(): return jnp.dot(hidden, w_down, preferred_element_type=F32)  13.8 us
    dot_general x2, matrix products, swiglu_rows(): gate_val = jnp.dot(row_set, w_gate, preferred_element_type=F32)  8.59 us
    all_to_all x2, local copies, waits for them, and re-layouts, per_device(): lax.all_to_all(send, ('sp', 'tp'), split_axis=0, concat_axis=0, tiled=True)  8.04 us
    pallas_call x1, Pallas kernels, attention(): pl.pallas_call(attention_kernel, out_shape=jax.ShapeDtypeStruct((rows, 25...  6.71 us
  transfers between devices with their start and end apart: 3, of which 3 were waited for; matrix products, arithmetic and copies ran while one was open for 2% of the time, Pallas kernels for 0%

profile of v1, /device:TPU:1, one launch (start us, length us, event | category | flops | bytes accessed | tf_op | source)
XLA Modules:
  0.0 259.3 jit_solution(6029415257330668199)
XLA Ops:
  6.5 0.0 copy-start
  6.5 0.0 all-gather.3.cloned.1.call-start
  6.5 1.1 copy.61
  7.6 1.0 copy.62
  8.6 1.6 maximum_maximum_fusion
  10.3 0.0 all-gather.3.cloned.1.call-update
  11.6 0.1 pad.9.clone
  11.7 0.1 pad_maximum_fusion.1.lam_ref
  11.8 0.8 select_reduce_fusion
  12.6 0.2 fusion.44
  12.8 1.0 fusion.57
  13.8 1.0 pad_maximum_fusion.q_ref
  14.8 0.0 copy-start.1
  14.8 63.4 %all-gather.3.cloned.1.call-done = bf16[8192,640]{0,1:T(8,128)(2,1)} async-done(((bf16[256,640]{0,1:T(8,128)(2,1)}), bf16[8192,640]{0,1:T(8,128)(2,1)}) %all-gather.3.cloned.1.call-update) | async-done | bytes 10485776 | tf_op jit(solution)/shard_map/all_gather | solution.py:170
  78.2 14.4 %copy.63 = bf16[8192,640]{1,0:T(8,128)(2,1)} copy(bf16[8192,640]{0,1:T(8,128)(2,1)} %all-gather.3.cloned.1.call-done) | data formatting | bytes 20971520 | tf_op jit(solution)/shard_map/all_gather | solution.py:170
  92.6 0.0 copy-done.1
  92.6 0.0 copy-start.2
  92.6 6.7 %shard_map.190 = bf16[256,256]{1,0:T(8,128)(2,1)} custom-call(bf16[256,512]{1,0:T(8,128)(2,1)S(1)} %pad_maximum_fusion.q_ref, bf16[32,256,640]{2,1,0:T(8,128)(2,1)} %bitcast.54, f32[2]{0:T(128)S(1)} %pad_maximum_fusion.1.lam_ref, f32[1,128]{1,0:T(1,128)S(1)} %bitcast.53), custom_call_target="tpu_custom_call" | custom-call | tf_op jit(solution)/shard_map/pallas_call | solution.py:84
  99.3 4.0 %all-to-all-start = ((bf16[4,64,256]{2,1,0:T(8,128)(2,1)}), bf16[4,64,256]{2,1,0:T(8,128)(2,1)S(1)}, u32[]{:S(2)}, u32[]{:S(2)}) async-start(bf16[4,64,256]{2,1,0:T(8,128)(2,1)} %bitcast.10), calls=%async_computation | async-start | bytes 262144 | tf_op jit(solution)/shard_map/all_to_all | solution.py:173
  103.3 0.1 eq.55
  103.4 0.1 copy.71
  103.5 0.1 copy.70
  103.6 4.5 %all-to-all-done = bf16[4,64,256]{2,1,0:T(8,128)(2,1)S(1)} async-done(((bf16[4,64,256]{2,1,0:T(8,128)(2,1)}), bf16[4,64,256]{2,1,0:T(8,128)(2,1)S(1)}, u32[]{:S(2)}, u32[]{:S(2)}) %all-to-all-start) | async-done | bytes 131104 | tf_op jit(solution)/shard_map/all_to_all | solution.py:173
  108.2 0.0 copy-done.2
  108.2 0.0 copy-start.3
  108.2 3.2 %multiply_reduce_fusion = (f32[64]{0:T(128)S(1)}, f32[64,2048]{1,0:T(8,128)S(1)}) fusion(bf16[1024,2048]{1,0:T(8,128)(2,1)} %param.30, bf16[64,512]{1,0:T(8,128)(2,1)S(1)} %get-tuple-element.13, bf16[64,512]{1,0:T(8,128)(2,1)S(1)} %get-tuple-element.14, bf16[64,2048]{1,0:T(8,128)(2,1)S(1)} %copy-done.2), kind=kOutput, calls=%fused_computation.23 | convolution fusion | flops 269483968 | bytes 5112064 | tf_op jit(solution)/shard_map/dot_general | solution.py:179
  111.4 0.1 and.16.clone
  111.5 0.0 copy-done.3
  111.5 2.1 convolution_convert_fusion
  113.6 4.1 %all_to_all.18 = bf16[128,4,2048]{2,1,0:T(4,128)(2,1)} reshape(bf16[512,2048]{1,0:T(8,128)(2,1)} %convolution_convert_fusion) | data formatting | bytes 4194304 | tf_op jit(solution)/shard_map/all_to_all | solution.py:190
  117.7 63.0 %all_to_all.26 = bf16[128,4,2048]{2,1,0:T(4,128)(2,1)} all-to-all(bf16[128,4,2048]{2,1,0:T(4,128)(2,1)} %all_to_all.18), channel_id=1, replica_groups=mesh['sp'=32,'tp'=4] {'sp','tp'}, dimensions={0} | all-to-all | bytes 4194304 | tf_op jit(solution)/shard_map/all_to_all | solution.py:190
  180.7 3.9 %all_to_all.20 = bf16[512,2048]{1,0:T(8,128)(2,1)} reshape(bf16[128,4,2048]{2,1,0:T(4,128)(2,1)} %all_to_all.26) | data formatting | bytes 4194304 | tf_op jit(solution)/shard_map/all_to_all | solution.py:190
  184.7 6.5 %fusion.4 = f32[512,1024]{1,0:T(8,128)} fusion(bf16[512,2048]{1,0:T(8,128)(2,1)} %all_to_all.20, bf16[1,2048,1024]{2,1,0:T(8,128)(2,1)} %param.34), kind=kOutput, calls=%fused_computation.4 | convolution fusion | flops 2147483648 | bytes 8388608 | tf_op jit(solution)/shard_map/dot_general | solution.py:103
  191.1 10.5 %fusion.6 = bf16[512,2048]{1,0:T(8,128)(2,1)} fusion(bf16[1,1024,2048]{2,1,0:T(8,128)(2,1)} %param.36, f32[512,1024]{1,0:T(8,128)} %fusion.4, bf16[512,2048]{1,0:T(8,128)(2,1)} %all_to_all.20, bf16[1,2048,1024]{2,1,0:T(8,128)(2,1)} %param.35), kind=kOutput, calls=%fused_computation.6 | convolution fusion | flops 4299161600 | bytes 14680064 | tf_op jit(solution)/shard_map/dot_general | solution.py:106
  201.7 4.1 %all_to_all.21 = bf16[128,4,2048]{2,1,0:T(4,128)(2,1)} reshape(bf16[512,2048]{1,0:T(8,128)(2,1)} %fusion.6) | data formatting | bytes 4194304 | tf_op jit(solution)/shard_map/all_to_all | solution.py:192
  205.8 4.9 %all-to-all-start.2 = ((bf16[128,4,2048]{2,1,0:T(4,128)(2,1)}), bf16[128,4,2048]{2,1,0:T(4,128)(2,1)}, u32[]{:S(2)}, u32[]{:S(2)}) async-start(bf16[128,4,2048]{2,1,0:T(4,128)(2,1)} %all_to_all.21), calls=%async_computation.2 | async-start | bytes 4194304 | tf_op jit(solution)/shard_map/all_to_all | solution.py:192
  210.7 2.1 fusion.56
  212.8 28.4 %all-to-all-done.2 = bf16[128,4,2048]{2,1,0:T(4,128)(2,1)} async-done(((bf16[128,4,2048]{2,1,0:T(4,128)(2,1)}), bf16[128,4,2048]{2,1,0:T(4,128)(2,1)}, u32[]{:S(2)}, u32[]{:S(2)}) %all-to-all-start.2) | async-done | bytes 2097184 | tf_op jit(solution)/shard_map/all_to_all | solution.py:192
  241.2 4.0 %convolution_bitcast_fusion.1 = f32[64,2048]{1,0:T(8,128)S(1)} fusion(bf16[128,4,2048]{2,1,0:T(4,128)(2,1)} %all-to-all-done.2, f32[64,128]{1,0:T(8,128)S(1)} %get-tuple-element.5, f32[64,128]{1,0:T(8,128)S(1)} %fusion.44, pred[64,128]{1,0:T(8,128)(4,1)S(1)} %broadcast_compare_fusion), kind=kOutput, calls=%fused_computation.13 | convolution fusion | flops 134316032 | bytes 2695168 | tf_op jit(solution)/shard_map/dot_general | solution.py:195
  245.2 4.0 %fusion.10 = f32[64,2048]{1,0:T(8,128)S(1)} fusion(f32[64,2048]{1,0:T(8,128)S(1)} %convolution_bitcast_fusion.1, bf16[128,4,2048]{2,1,0:T(4,128)(2,1)} %all-to-all-done.2, f32[64,128]{1,0:T(8,128)S(1)} %get-tuple-element.5, f32[64,128]{1,0:T(8,128)S(1)} %fusion.44, pred[64,128]{1,0:T(8,128)(4,1)S(1)} %broadcast_compare_fusion), kind=kOutput, calls=%fused_computation.12 | convolution fusion | flops 134578176 | bytes 3219456 | tf_op jit(solution)/shard_map/dot_general | solution.py:195
  249.2 0.0 copy-done
  249.2 3.3 %fusion.11 = bf16[64,2048]{1,0:T(8,128)(2,1)} fusion(f32[64,2048]{1,0:T(8,128)S(1)} %fusion.10, f32[64,2048]{1,0:T(8,128)S(1)} %get-tuple-element.12, bf16[512,2048]{1,0:T(8,128)(2,1)S(1)} %copy-done, bf16[2048,512]{1,0:T(8,128)(2,1)} %param.38, f32[64,512]{1,0:T(8,128)S(1)} %fusion.56, f32[2048]{0:T(1024)S(1)} %copy-done.3, f32[64]{0:T(128)S(1)} %add_rsqrt_fusion), kind=kOutput, calls=%fused_computation.14 | convolution fusion | flops 269418496 | bytes 5644544 | tf_op jit(solution)/shard_map/dot_general | solution.py:106
  (8 shorter events, 0.1 us)
Async XLA Ops:
  6.5 242.6 %copy-start = (bf16[512,2048]{1,0:T(8,128)(2,1)S(1)}, bf16[512,2048]{1,0:T(8,128)(2,1)}, u32[]{:S(2)}) copy-start(bf16[512,2048]{1,0:T(8,128)(2,1)} %param.39) | copy-start | bytes 6291460
  6.5 71.7 %all-gather.3.cloned.1.call-start = ((), (), s32[]{:S(2)}) async-start(), calls=%async_computation.3 | async-start | bytes 10813440 | tf_op jit(solution)/shard_map/all_gather | solution.py:170
  14.8 77.8 %copy-start.1 = (f32[128]{0:T(128)S(1)}, f32[128]{0:T(128)}, u32[]{:S(2)}) copy-start(f32[128]{0:T(128)} %param.29) | copy-start | bytes 1540
  92.6 15.6 %copy-start.2 = (bf16[64,2048]{1,0:T(8,128)(2,1)S(1)}, bf16[64,2048]{1,0:T(8,128)(2,1)}, u32[]{:S(2)}) copy-start(bf16[64,2048]{1,0:T(8,128)(2,1)} %param.20) | copy-start | bytes 786436
  99.3 8.8 %all-to-all-start = ((bf16[4,64,256]{2,1,0:T(8,128)(2,1)}), bf16[4,64,256]{2,1,0:T(8,128)(2,1)S(1)}, u32[]{:S(2)}, u32[]{:S(2)}) async-start(bf16[4,64,256]{2,1,0:T(8,128)(2,1)} %bitcast.10), calls=%async_computation | async-start | bytes 262144 | tf_op jit(solution)/shard_map/all_to_all | solution.py:173
  108.2 3.3 %copy-start.3 = (f32[2048]{0:T(1024)S(1)}, f32[2048]{0:T(1024)}, u32[]{:S(2)}) copy-start(f32[2048]{0:T(1024)} %param.31) | copy-start | bytes 24580
  205.8 35.4 %all-to-all-start.2 = ((bf16[128,4,2048]{2,1,0:T(4,128)(2,1)}), bf16[128,4,2048]{2,1,0:T(4,128)(2,1)}, u32[]{:S(2)}, u32[]{:S(2)}) async-start(bf16[128,4,2048]{2,1,0:T(4,128)(2,1)} %all_to_all.21), calls=%async_computation.2 | async-start | bytes 4194304 | tf_op jit(solution)/shard_map/all_to_all | solution.py:192
Sparse Core Ops, SparseCore 0:
  10.4 67.7 all-gather.2

commit v2 on v1

--- a/solution.py
+++ b/solution.py
@@ -20,19 +20,108 @@
     return lax.dot_general(a, b, (((1,), (1,)), ((), ())), preferred_element_type=F32)
 
 
-def attention_kernel(q_ref, kv_ref, lam_ref, gain_ref, out_ref, acc, top):
-    me = lax.axis_index("sp")
-    chip = me // 2
+MESH = pl.DeviceIdType.MESH
+SIDE = 4
+
+
+def attention_kernel(
+    q_ref, own_ref, lam_ref, gain_ref, out_ref, kv, heads, acc, top, send_sem, half_sem, pair_sem, tp_send, tp_recv
+):
+    sp = lax.axis_index("sp")
+    tp = lax.axis_index("tp")
+    core = sp % 2
+    chip = sp // 2
+    z = chip // SIDE
+    y = chip % SIDE
     rows = q_ref.shape[0]
+    half = rows // 2
     ones = jnp.ones((8, 2 * rows), BF16)
     scale_a = LOG2E * 64**-0.5
     scale_b = LOG2E * 128**-0.5
 
+    def at(zz, yy, cc):
+        return ((zz % SIDE) * SIDE + yy % SIDE) * 2 + cc
+
+    def neighbour(dim, step):
+        return (at(z + step, y, core), tp) if dim == 0 else (at(z, y + step, core), tp)
+
+    partner = (at(z, y, 1 - core), tp)
+    barrier = pltpu.get_barrier_semaphore()
+    peers = [neighbour(d, s) for d in (0, 1) for s in (1, 3)] + [partner]
+    peers += [(sp, (tp + k) % 4) for k in (1, 2, 3)]
+    for peer in peers:
+        pl.semaphore_signal(barrier, inc=1, device_id=peer, device_id_type=MESH)
+    pl.semaphore_wait(barrier, len(peers))
+
+    started = []
+
+    def dims(h):
+        return (1, 0) if h == 0 else (0, 1)
+
+    def piece_of(h, o1, o2):
+        return at(z - o2, y - o1, core) if h == 0 else at(z - o1, y - o2, core)
+
+    def half_send(h, o1, o2, along, step, part=None):
+        dim = dims(h)[along]
+        new = [o1, o2]
+        new[along] = (new[along] + step) % SIDE
+        lo, size = (h * half, half) if part is None else (h * half + part * half // 2, half // 2)
+        p = piece_of(h, o1, o2)
+        own = o1 == 0 and o2 == 0
+        source = own_ref.at[pl.ds(lo, size)] if own else kv.at[p, pl.ds(lo, size)]
+        copy = pltpu.make_async_remote_copy(
+            src_ref=source,
+            dst_ref=kv.at[p, pl.ds(lo, size)],
+            send_sem=send_sem.at[len(started)],
+            recv_sem=half_sem.at[h * 16 + new[0] * 4 + new[1]],
+            device_id=neighbour(dim, step),
+            device_id_type=MESH,
+        )
+        copy.start()
+        started.append(copy)
+
+    def half_wait(h, o1, o2):
+        p = piece_of(h, o1, o2)
+        pltpu.make_async_copy(
+            kv.at[p, pl.ds(h * half, half)],
+            kv.at[p, pl.ds(h * half, half)],
+            half_sem.at[h * 16 + o1 * 4 + o2],
+        ).wait()
+
+    def spread(h, o1, o2, along):
+        o = (o1, o2)[along]
+        if o == 0:
+            half_send(h, o1, o2, along, 1)
+            half_send(h, o1, o2, along, 3)
+        elif o == 1:
+            half_send(h, o1, o2, along, 1, 0)
+        elif o == 3:
+            half_send(h, o1, o2, along, 3, 1)
+
+    def arrive(h, o1, o2):
+        half_wait(h, o1, o2)
+        if o2 == 0:
+            spread(h, o1, o2, 0)
+        spread(h, o1, o2, 1)
+
+    def pair_send(a, b):
+        p = at(z - a, y - b, core)
+        copy = pltpu.make_async_remote_copy(
+            src_ref=own_ref if (a, b) == (0, 0) else kv.at[p],
+            dst_ref=kv.at[p],
+            send_sem=send_sem.at[len(started)],
+            recv_sem=pair_sem.at[a * 4 + b],
+            device_id=partner,
+            device_id_type=MESH,
+        )
+        copy.start()
+        started.append(copy)
+
     def chunk(c, masked, first):
-        piece = [kv_ref.at[2 * c], kv_ref.at[2 * c + 1]]
+        piece = [kv.at[2 * c], kv.at[2 * c + 1]]
         if masked:
             key_pos = lax.broadcasted_iota(jnp.int32, (2 * rows, rows), 0)
-            query_pos = lax.broadcasted_iota(jnp.int32, (2 * rows, rows), 1) + (me % 2) * rows
+            query_pos = lax.broadcasted_iota(jnp.int32, (2 * rows, rows), 1) + core * rows
             keep = key_pos <= query_pos
         for head in range(2):
             vt = jnp.concatenate(
@@ -59,13 +148,73 @@
                     acc[h] = acc[h] * jnp.exp2(old - best) + add
                 top[h : h + 1, :] = best
 
+    def chunks(offsets):
+        code = 0
+        for k, (a, b) in enumerate(offsets):
+            code += (a * 4 + b) * 16**k
+
+        def body(k, left):
+            o = left % 16
+            a = o // 4
+            b = o % 4
+            p = at(z - a, y - b, 1 - core)
+            pltpu.make_async_copy(kv.at[p], kv.at[p], pair_sem.at[o]).wait()
+            c = p // 2
+
+            @pl.when(c < chip)
+            def _():
+                chunk(c, False, False)
+
+            return left // 16
+
+        lax.fori_loop(0, len(offsets), body, jnp.int32(code))
+
+    for h in range(2):
+        spread(h, 0, 0, 0)
+    pair_send(0, 0)
+    for h in range(2):
+        spread(h, 0, 0, 1)
+    kv[sp] = own_ref[...]
+    pltpu.make_async_copy(kv.at[sp], kv.at[sp], pair_sem.at[0]).wait()
     chunk(chip, True, True)
 
-    def body(c, carry):
-        chunk(c, False, False)
-        return carry
-
-    lax.fori_loop(0, chip, body, 0)
+    for o1 in (1, 3):
+        for h in range(2):
+            arrive(h, o1, 0)
+    for o2 in (1, 3):
+        for h in range(2):
+            arrive(h, 0, o2)
+    near = [(0, 1), (0, 3), (1, 0), (3, 0)]
+    for a, b in near:
+        pair_send(a, b)
+    chunks(near)
+    for h in range(2):
+        arrive(h, 2, 0)
+    for o1 in (1, 3):
+        for o2 in (1, 3):
+            for h in range(2):
+                arrive(h, o1, o2)
+    for h in range(2):
+        arrive(h, 0, 2)
+    second = [(0, 2), (2, 0), (1, 1), (1, 3), (3, 1), (3, 3)]
+    for a, b in second:
+        pair_send(a, b)
+    chunks(second[:3])
+    for o2 in (1, 3):
+        for h in range(2):
+            arrive(h, 2, o2)
+    for o1 in (1, 3):
+        for h in range(2):
+            arrive(h, o1, 2)
+    third = [(1, 2), (3, 2), (2, 1), (2, 3)]
+    for a, b in third:
+        pair_send(a, b)
+    chunks(second[3:])
+    for h in range(2):
+        arrive(h, 2, 2)
+    pair_send(2, 2)
+    chunks(third + [(2, 2)])
+
     for head in range(2):
         first = acc[2 * head]
         second = acc[2 * head + 1]
@@ -73,17 +222,35 @@
         two = second[0:128] / second[128:129]
         differ = one - lam_ref[head] * two
         scale = lax.rsqrt(jnp.mean(differ * differ, axis=0, keepdims=True) + EPSILON)
-        heads = differ * scale
-        out_ref[:, head * 128 : head * 128 + 128] = (
-            heads.T * gain_ref[...] * HEAD_SCALE
-        ).astype(BF16)
-
-
-def attention(q, kv, lam, gain):
+        done = (differ * scale).T * gain_ref[...] * HEAD_SCALE
+        heads[:, :, head * 128 : head * 128 + 128] = done.astype(BF16).reshape(4, rows // 4, 128)
+    sends = []
+    for k in (1, 2, 3):
+        to = (tp + k) % 4
+        copy = pltpu.make_async_remote_copy(
+            src_ref=heads.at[to],
+            dst_ref=out_ref.at[tp],
+            send_sem=tp_send.at[k],
+            recv_sem=tp_recv.at[k],
+            device_id=(sp, to),
+            device_id_type=MESH,
+        )
+        copy.start()
+        sends.append(copy)
+    out_ref[tp] = heads[tp]
+    for copy in started:
+        copy.wait_send()
+    for k in (1, 2, 3):
+        sends[k - 1].wait_send()
+        source = (tp + 4 - k) % 4
+        pltpu.make_async_copy(out_ref.at[source], out_ref.at[source], tp_recv.at[k]).wait()
+
+
+def attention(q, piece, lam, gain):
     rows = q.shape[0]
     return pl.pallas_call(
         attention_kernel,
-        out_shape=jax.ShapeDtypeStruct((rows, 256), BF16),
+        out_shape=jax.ShapeDtypeStruct((4, rows // 4, 256), BF16),
         in_specs=[
             pl.BlockSpec(memory_space=pltpu.VMEM),
             pl.BlockSpec(memory_space=pltpu.VMEM),
@@ -92,11 +259,20 @@
         ],
         out_specs=pl.BlockSpec(memory_space=pltpu.VMEM),
         scratch_shapes=[
+            pltpu.VMEM((32, rows, 640), BF16),
+            pltpu.VMEM((4, rows // 4, 256), BF16),
             pltpu.VMEM((4, 136, rows), F32),
             pltpu.VMEM((8, rows), F32),
+            pltpu.SemaphoreType.DMA((64,)),
+            pltpu.SemaphoreType.DMA((32,)),
+            pltpu.SemaphoreType.DMA((16,)),
+            pltpu.SemaphoreType.DMA((4,)),
+            pltpu.SemaphoreType.DMA((4,)),
         ],
-        compiler_params=pltpu.CompilerParams(vmem_limit_bytes=48 * 1024 * 1024),
-    )(q, kv, lam, gain)
+        compiler_params=pltpu.CompilerParams(
+            vmem_limit_bytes=48 * 1024 * 1024, collective_id=0, has_side_effects=True
+        ),
+    )(q, piece, lam, gain)
 
 
 def swiglu_rows(row_set, w_gate, w_up, w_down):
@@ -167,12 +343,8 @@
         ],
         axis=1,
     )
-    kv = lax.all_gather(piece, "sp", axis=0, tiled=False)
     lam = jnp.concatenate([lambda_a, lambda_b])
-    heads = attention(q, kv, lam, head_gain[None, :])
-    back = lax.all_to_all(
-        heads.reshape(tp_count, tok_dev, 256), "tp", split_axis=0, concat_axis=0, tiled=True
-    )
+    back = attention(q, piece, lam, head_gain[None, :])
     joined = jnp.concatenate(
         [back[:, :, :128].transpose(1, 0, 2).reshape(tok_dev, -1),
          back[:, :, 128:].transpose(1, 0, 2).reshape(tok_dev, -1)], axis=1)

time: 261 us -> 181 us (0.69)
  waiting for transfers between devices: 96.2 us -> 28.4 us
  Pallas kernels: 6.71 us -> 42.8 us
  blocking collectives: 63 us -> 48.5 us
  local copies, waits for them, and re-layouts: 30.2 us -> 16.4 us
  between operations: 14.9 us -> 1.53 us
  starting transfers between devices: 8.86 us -> 4.84 us
    all_gather x1 -> x0, waiting for transfers between devices: 63.4 us -> none  [per_device(): kv = lax.all_gather(piece, 'sp', axis=0, tiled=False)]
    pallas_call x1, Pallas kernels: 6.71 us -> 42.8 us  [attention(): pl.pallas_call(attention_kernel, out_shape=jax.ShapeDtypeStruct((4, rows...]
    all_to_all x1, blocking collectives: 63 us -> 48.5 us  [per_device(): lax.all_to_all(send, ('sp', 'tp'), split_axis=0, concat_axis=0, tiled=True)]
    all_gather x1 -> x0, local copies, waits for them, and re-layouts: 14.4 us -> none  [per_device(): kv = lax.all_gather(piece, 'sp', axis=0, tiled=False)]
    all_to_all x1 -> x0, waiting for transfers between devices: 4.47 us -> none  [per_device(): lax.all_to_all(heads.reshape(tp_count, tok_dev, 256), 'tp', split_axis=0,...]
    all_to_all x1 -> x0, starting transfers between devices: 3.97 us -> none  [per_device(): lax.all_to_all(heads.reshape(tp_count, tok_dev, 256), 'tp', split_axis=0,...]
  transfers between devices with their start and end apart: 3 -> 1, of which waited for: 3 -> 1; matrix products, arithmetic and copies ran while one was open for 2% -> 1% of each run, Pallas kernels for 0% -> 0%
where the time goes in v2:
time: 181 us; the launch traced here: 180 us
  blocking collectives  48.5 us (27%)
  Pallas kernels  42.8 us (24%)
  matrix products  35.8 us (20%)
  waiting for transfers between devices  28.4 us (16%)
  local copies, waits for them, and re-layouts  16.4 us (9%)
  starting transfers between devices  4.84 us (3%)
  other arithmetic  2.19 us (1%)
    all_to_all x1, blocking collectives, per_device(): lax.all_to_all(send, ('sp', 'tp'), split_axis=0, concat_axis=0, tiled=True)  48.5 us
    pallas_call x1, Pallas kernels, attention(): pl.pallas_call(attention_kernel, out_shape=jax.ShapeDtypeStruct((4, rows...  42.8 us
    all_to_all x1, waiting for transfers between devices, per_device(): lax.all_to_all(result, ('sp', 'tp'), split_axis=0, concat_axis=0, tiled=T...  28.4 us
    dot_general x2, matrix products, swiglu_rows(): return jnp.dot(hidden, w_down, preferred_element_type=F32)  13.8 us
    dot_general x2, matrix products, swiglu_rows(): gate_val = jnp.dot(row_set, w_gate, preferred_element_type=F32)  8.59 us
    all_to_all x2, local copies, waits for them, and re-layouts, per_device(): lax.all_to_all(send, ('sp', 'tp'), split_axis=0, concat_axis=0, tiled=True)  8.03 us
    all_to_all x1, starting transfers between devices, per_device(): lax.all_to_all(result, ('sp', 'tp'), split_axis=0, concat_axis=0, tiled=T...  4.84 us
    all_to_all x1, local copies, waits for them, and re-layouts, per_device(): lax.all_to_all(result, ('sp', 'tp'), split_axis=0, concat_axis=0, tiled=T...  4.09 us
  transfers between devices with their start and end apart: 1, of which 1 were waited for; matrix products, arithmetic and copies ran while one was open for 1% of the time, Pallas kernels for 0%

profile of v2, /device:TPU:1, one launch (start us, length us, event | category | flops | bytes accessed | tf_op | source)
XLA Modules:
  0.0 180.5 jit_solution(17166350202526551259)
XLA Ops:
  0.0 0.0 copy-start
  0.0 0.0 copy-start.2
  0.0 1.1 fusion.57
  1.1 0.9 copy.58
  2.1 0.9 copy.59
  4.3 0.1 pad.9.clone
  4.4 0.1 pad_maximum_fusion.1.lam_ref
  4.5 1.0 pad_maximum_fusion.q_ref
  5.5 0.9 maximum_maximum_fusion.own_ref
  6.5 0.0 copy-start.1
  6.5 0.6 copy-done.1
  7.1 42.8 %shard_map.190 = bf16[4,64,256]{2,1,0:T(8,128)(2,1)S(1)} custom-call(bf16[256,512]{1,0:T(8,128)(2,1)S(1)} %pad_maximum_fusion.q_ref, bf16[256,640]{1,0:T(8,128)(2,1)S(1)} %maximum_maximum_fusion.own_ref, f32[2]{0:T(128)S(1)} %pad_maximum_fusion.1.lam_ref, f32[1,128]{1,0:T(1,128)S(1)} %bitcast.51), custom_call_target="tpu_custom_call" | custom-call | tf_op jit(solution)/shard_map/pallas_call | solution.py:251
  50.0 0.0 copy-done.2
  50.0 0.0 copy-start.4
  50.0 0.0 copy-start.5
  50.0 0.0 copy-start.3
  50.0 3.2 %multiply_reduce_fusion = (f32[64]{0:T(128)S(1)}, f32[64,2048]{1,0:T(8,128)S(1)}) fusion(bf16[1024,2048]{1,0:T(8,128)(2,1)} %param.30, bf16[64,512]{1,0:T(8,128)(2,1)S(1)} %get-tuple-element.13, bf16[64,512]{1,0:T(8,128)(2,1)S(1)} %get-tuple-element.14, bf16[64,2048]{1,0:T(8,128)(2,1)S(1)} %copy-done.2), kind=kOutput, calls=%fused_computation.23 | convolution fusion | flops 269483968 | bytes 5112064 | tf_op jit(solution)/shard_map/dot_general | solution.py:351
  53.2 0.0 copy-done.4
  53.3 0.0 copy-done.5
  53.3 0.1 select_reduce_fusion
  53.4 0.2 fusion.44
  53.6 0.1 copy.66
  53.7 0.1 copy.67
  53.9 0.1 eq.55
  54.0 0.1 and.16.clone
  54.1 0.0 copy-done.3
  54.1 2.1 %convolution_convert_fusion = bf16[512,2048]{1,0:T(8,128)(2,1)} fusion(pred[64,512]{0,1:T(8,128)(4,1)S(1)} %bitcast.53, f32[64,512]{0,1:T(8,128)S(1)} %bitcast.52, f32[512]{0:T(512)S(1)} %eq.55, f32[64,2048]{1,0:T(8,128)S(1)} %get-tuple-element.12, f32[2048]{0:T(1024)S(1)} %copy-done.3, f32[64]{0:T(128)S(1)} %add_rsqrt_fusion), kind=kOutput, calls=%fused_computation.7 | convolution fusion | flops 135725056 | bytes 2795776 | tf_op jit(solution)/shard_map/dot_general | solution.py:361
  56.2 4.1 %all_to_all.14 = bf16[128,4,2048]{2,1,0:T(4,128)(2,1)} reshape(bf16[512,2048]{1,0:T(8,128)(2,1)} %convolution_convert_fusion) | data formatting | bytes 4194304 | tf_op jit(solution)/shard_map/all_to_all | solution.py:362
  60.3 48.5 %all_to_all.21 = bf16[128,4,2048]{2,1,0:T(4,128)(2,1)} all-to-all(bf16[128,4,2048]{2,1,0:T(4,128)(2,1)} %all_to_all.14), channel_id=1, replica_groups=mesh['sp'=32,'tp'=4] {'sp','tp'}, dimensions={0} | all-to-all | bytes 4194304 | tf_op jit(solution)/shard_map/all_to_all | solution.py:362
  108.8 3.9 %all_to_all.16 = bf16[512,2048]{1,0:T(8,128)(2,1)} reshape(bf16[128,4,2048]{2,1,0:T(4,128)(2,1)} %all_to_all.21) | data formatting | bytes 4194304 | tf_op jit(solution)/shard_map/all_to_all | solution.py:362
  112.7 6.5 %fusion.4 = f32[512,1024]{1,0:T(8,128)} fusion(bf16[512,2048]{1,0:T(8,128)(2,1)} %all_to_all.16, bf16[1,2048,1024]{2,1,0:T(8,128)(2,1)} %param.34), kind=kOutput, calls=%fused_computation.4 | convolution fusion | flops 2147483648 | bytes 8388608 | tf_op jit(solution)/shard_map/dot_general | solution.py:279
  119.2 10.5 %fusion.6 = bf16[512,2048]{1,0:T(8,128)(2,1)} fusion(bf16[1,1024,2048]{2,1,0:T(8,128)(2,1)} %param.36, f32[512,1024]{1,0:T(8,128)} %fusion.4, bf16[512,2048]{1,0:T(8,128)(2,1)} %all_to_all.16, bf16[1,2048,1024]{2,1,0:T(8,128)(2,1)} %param.35), kind=kOutput, calls=%fused_computation.6 | convolution fusion | flops 4299161600 | bytes 14680064 | tf_op jit(solution)/shard_map/dot_general | solution.py:282
  129.8 4.1 %all_to_all.17 = bf16[128,4,2048]{2,1,0:T(4,128)(2,1)} reshape(bf16[512,2048]{1,0:T(8,128)(2,1)} %fusion.6) | data formatting | bytes 4194304 | tf_op jit(solution)/shard_map/all_to_all | solution.py:364
  133.8 4.8 %all-to-all-start.1 = ((bf16[128,4,2048]{2,1,0:T(4,128)(2,1)}), bf16[128,4,2048]{2,1,0:T(4,128)(2,1)}, u32[]{:S(2)}, u32[]{:S(2)}) async-start(bf16[128,4,2048]{2,1,0:T(4,128)(2,1)} %all_to_all.17), calls=%async_computation.1 | async-start | bytes 4194304 | tf_op jit(solution)/shard_map/all_to_all | solution.py:364
  138.7 2.1 %fusion.56 = f32[64,512]{1,0:T(8,128)S(1)} fusion(bf16[2048,512]{1,0:T(8,128)(2,1)} %param.37, f32[64,2048]{1,0:T(8,128)S(1)} %get-tuple-element.12, f32[2048]{0:T(1024)S(1)} %copy-done.3, f32[64]{0:T(128)S(1)} %add_rsqrt_fusion), kind=kOutput, calls=%fused_computation.75 | convolution fusion | flops 134610944 | bytes 2760960 | tf_op jit(solution)/shard_map/dot_general | solution.py:279
  140.8 28.4 %all-to-all-done.1 = bf16[128,4,2048]{2,1,0:T(4,128)(2,1)} async-done(((bf16[128,4,2048]{2,1,0:T(4,128)(2,1)}), bf16[128,4,2048]{2,1,0:T(4,128)(2,1)}, u32[]{:S(2)}, u32[]{:S(2)}) %all-to-all-start.1) | async-done | bytes 2097184 | tf_op jit(solution)/shard_map/all_to_all | solution.py:364
  169.2 4.0 %convolution_bitcast_fusion.1 = f32[64,2048]{1,0:T(8,128)S(1)} fusion(bf16[128,4,2048]{2,1,0:T(4,128)(2,1)} %all-to-all-done.1, f32[64,128]{1,0:T(8,128)S(1)} %get-tuple-element.5, f32[64,128]{1,0:T(8,128)S(1)} %fusion.44, pred[64,128]{1,0:T(8,128)(4,1)S(1)} %broadcast_compare_fusion), kind=kOutput, calls=%fused_computation.13 | convolution fusion | flops 134316032 | bytes 2695168 | tf_op jit(solution)/shard_map/dot_general | solution.py:367
  173.2 4.0 %fusion.10 = f32[64,2048]{1,0:T(8,128)S(1)} fusion(f32[64,2048]{1,0:T(8,128)S(1)} %convolution_bitcast_fusion.1, bf16[128,4,2048]{2,1,0:T(4,128)(2,1)} %all-to-all-done.1, f32[64,128]{1,0:T(8,128)S(1)} %get-tuple-element.5, f32[64,128]{1,0:T(8,128)S(1)} %fusion.44, pred[64,128]{1,0:T(8,128)(4,1)S(1)} %broadcast_compare_fusion), kind=kOutput, calls=%fused_computation.12 | convolution fusion | flops 134578176 | bytes 3219456 | tf_op jit(solution)/shard_map/dot_general | solution.py:367
  177.2 0.0 copy-done
  177.2 3.3 %fusion.11 = bf16[64,2048]{1,0:T(8,128)(2,1)} fusion(f32[64,2048]{1,0:T(8,128)S(1)} %fusion.10, f32[64,2048]{1,0:T(8,128)S(1)} %get-tuple-element.12, bf16[512,2048]{1,0:T(8,128)(2,1)S(1)} %copy-done, bf16[2048,512]{1,0:T(8,128)(2,1)} %param.38, f32[64,512]{1,0:T(8,128)S(1)} %fusion.56, f32[2048]{0:T(1024)S(1)} %copy-done.3, f32[64]{0:T(128)S(1)} %add_rsqrt_fusion), kind=kOutput, calls=%fused_computation.14 | convolution fusion | flops 269418496 | bytes 5644544 | tf_op jit(solution)/shard_map/dot_general | solution.py:282
  (8 shorter events, 0.1 us)
Async XLA Ops:
  0.0 177.2 %copy-start = (bf16[512,2048]{1,0:T(8,128)(2,1)S(1)}, bf16[512,2048]{1,0:T(8,128)(2,1)}, u32[]{:S(2)}) copy-start(bf16[512,2048]{1,0:T(8,128)(2,1)} %param.39) | copy-start | bytes 6291460
  0.0 50.0 %copy-start.2 = (bf16[64,2048]{1,0:T(8,128)(2,1)S(1)}, bf16[64,2048]{1,0:T(8,128)(2,1)}, u32[]{:S(2)}) copy-start(bf16[64,2048]{1,0:T(8,128)(2,1)} %param.20) | copy-start | bytes 786436
  6.5 0.7 copy-start.1
  50.0 3.2 %copy-start.4 = (f32[64,4]{0,1:T(4,128)S(1)}, f32[64,4]{0,1:T(4,128)}, u32[]{:S(2)}) copy-start(f32[64,4]{0,1:T(4,128)} %param.33) | copy-start | bytes 3076
  50.0 3.2 %copy-start.5 = (s32[64,4]{0,1:T(4,128)S(1)}, s32[64,4]{0,1:T(4,128)}, u32[]{:S(2)}) copy-start(s32[64,4]{0,1:T(4,128)} %param.32) | copy-start | bytes 3076
  50.0 4.1 %copy-start.3 = (f32[2048]{0:T(1024)S(1)}, f32[2048]{0:T(1024)}, u32[]{:S(2)}) copy-start(f32[2048]{0:T(1024)} %param.31) | copy-start | bytes 24580
  133.8 35.4 %all-to-all-start.1 = ((bf16[128,4,2048]{2,1,0:T(4,128)(2,1)}), bf16[128,4,2048]{2,1,0:T(4,128)(2,1)}, u32[]{:S(2)}, u32[]{:S(2)}) async-start(bf16[128,4,2048]{2,1,0:T(4,128)(2,1)} %all_to_all.17), calls=%async_computation.1 | async-start | bytes 4194304 | tf_op jit(solution)/shard_map/all_to_all | solution.py:364

commit v3 on v2

--- a/solution.py
+++ b/solution.py
@@ -1,8 +1,8 @@
-import functools
-import math
+import itertools
 
 import jax
 import jax.numpy as jnp
+import numpy as np
 from jax import lax
 from jax.experimental import pallas as pl
 from jax.experimental.pallas import tpu as pltpu
@@ -24,8 +24,81 @@
 SIDE = 4
 
 
-def attention_kernel(
-    q_ref, own_ref, lam_ref, gain_ref, out_ref, kv, heads, acc, top, send_sem, half_sem, pair_sem, tp_send, tp_recv
+def flows():
+    every = [(a, b, c) for a in range(SIDE) for b in range(SIDE) for c in range(SIDE)]
+    order, groups = [], []
+    for mask in itertools.product((0, 1), repeat=3):
+        if any(mask):
+            members = [o for o in every if tuple(int(v == 2) for v in o) == mask]
+            groups.append((mask, len(order), len(order) + len(members)))
+            order += [o + (1,) for o in members]
+    far = [o for o in every if 2 in o]
+    near = [o for o in every if 2 not in o]
+    order += [o + (1,) for o in near]
+    order += [o + (0,) for o in far]
+    order += [o + (0,) for o in near if any(o)] + [(0, 0, 0, 0)]
+    return order, groups
+
+
+ORDER, GROUPS = flows()
+RELAYED = GROUPS[-1][2]
+FAR_END = 64 + RELAYED
+
+
+def layer_kernel(
+    q_ref,
+    own_ref,
+    lam_ref,
+    gain_ref,
+    resid_ref,
+    norm_ref,
+    ids_ref,
+    mix_ref,
+    table_ref,
+    wo_hbm,
+    wg_hbm,
+    wu_hbm,
+    wd_hbm,
+    sg_hbm,
+    su_hbm,
+    sd_hbm,
+    out_ref,
+    kv,
+    heads,
+    back,
+    acc,
+    top,
+    wo,
+    wg,
+    wu,
+    wd,
+    sg,
+    su,
+    sd,
+    fill,
+    combine,
+    perm,
+    middle,
+    shared,
+    send,
+    recv,
+    res,
+    ret,
+    relay_out,
+    relay_back,
+    xs,
+    hs,
+    rs,
+    routed,
+    send_sem,
+    half_sem,
+    pair_sem,
+    tp_send,
+    tp_recv,
+    load_sem,
+    a2a_send,
+    a2a_recv,
+    relay_recv,
 ):
     sp = lax.axis_index("sp")
     tp = lax.axis_index("tp")
@@ -46,12 +119,26 @@
         return (at(z + step, y, core), tp) if dim == 0 else (at(z, y + step, core), tp)
 
     partner = (at(z, y, 1 - core), tp)
+    loads = [
+        pltpu.make_async_copy(source, target, load_sem.at[k])
+        for k, (source, target) in enumerate(
+            [(wo_hbm, wo), (sg_hbm, sg), (su_hbm, su), (sd_hbm, sd), (wg_hbm, wg), (wu_hbm, wu), (wd_hbm, wd)]
+        )
+    ]
+    for load in loads:
+        load.start()
+    me = sp * 4 + tp
     barrier = pltpu.get_barrier_semaphore()
-    peers = [neighbour(d, s) for d in (0, 1) for s in (1, 3)] + [partner]
-    peers += [(sp, (tp + k) % 4) for k in (1, 2, 3)]
-    for peer in peers:
-        pl.semaphore_signal(barrier, inc=1, device_id=peer, device_id_type=MESH)
-    pl.semaphore_wait(barrier, len(peers))
+
+    def greet(k, carry):
+        other = (me + k) % 128
+        pl.semaphore_signal(
+            barrier, inc=1, device_id=(other // 4, other % 4), device_id_type=MESH
+        )
+        return carry
+
+    lax.fori_loop(1, 128, greet, 0)
+    pl.semaphore_wait(barrier, 127)
 
     started = []
 
@@ -169,6 +256,43 @@
 
         lax.fori_loop(0, len(offsets), body, jnp.int32(code))
 
+    def slot_matrices():
+        lane = lax.broadcasted_iota(jnp.int32, (64, 2048), 1)
+        quarter = (lane // 4) % 4
+        oz, oy, ox, oc = (table_ref[k : k + 1, :] for k in range(4))
+        expert = at(z + oz, y + oy, (core + oc) % 2) * 4 + (tp + ox) % 4
+        named = jnp.zeros((64, 2048), F32)
+        mixed = jnp.zeros((64, 2048), F32)
+        for k in range(4):
+            same = ids_ref[:, k : k + 1] == expert
+            named = named + jnp.where(same, 1.0, 0.0)
+            mixed = mixed + jnp.where(same, mix_ref[:, k : k + 1], 0.0)
+        before = jnp.where(
+            lax.broadcasted_iota(jnp.int32, (64, 64), 1) < lax.broadcasted_iota(jnp.int32, (64, 64), 0),
+            1.0,
+            0.0,
+        ).astype(BF16)
+        rank = jnp.dot(before, named.astype(BF16), preferred_element_type=F32)
+        hit = (named > 0.5) & (jnp.abs(rank - (lane % 4).astype(F32)) < 0.5)
+        placed = jnp.where(hit, 1.0, 0.0)
+        mixed = jnp.where(hit, mixed, 0.0)
+        high = mixed.astype(BF16).astype(F32)
+        low = mixed - high
+        for j in range(4):
+            keep = quarter == j
+            combine[j * 64 : j * 64 + 64] = jnp.where(keep, high, 0.0).astype(BF16)
+            combine[256 + j * 64 : 256 + j * 64 + 64] = jnp.where(keep, low, 0.0).astype(BF16)
+        for k in range(8):
+            cols = slice(k * 256, k * 256 + 256)
+            block = jnp.concatenate(
+                [jnp.where(quarter[:, cols] == j, placed[:, cols], 0.0) for j in range(4)], axis=0
+            )
+            fill[cols] = block.T.astype(BF16)
+        a = lax.broadcasted_iota(jnp.int32, (256, 256), 0)
+        b = lax.broadcasted_iota(jnp.int32, (256, 256), 1)
+        perm[0] = jnp.where(b == ((a // 4) % 16) * 16 + (a // 64) * 4 + a % 4, 1.0, 0.0).astype(BF16)
+        perm[1] = jnp.where(a == ((b // 4) % 16) * 16 + (b // 64) * 4 + b % 4, 1.0, 0.0).astype(BF16)
+
     for h in range(2):
         spread(h, 0, 0, 0)
     pair_send(0, 0)
@@ -177,6 +301,8 @@
     kv[sp] = own_ref[...]
     pltpu.make_async_copy(kv.at[sp], kv.at[sp], pair_sem.at[0]).wait()
     chunk(chip, True, True)
+
+    slot_matrices()
 
     for o1 in (1, 3):
         for h in range(2):
@@ -229,7 +355,7 @@
         to = (tp + k) % 4
         copy = pltpu.make_async_remote_copy(
             src_ref=heads.at[to],
-            dst_ref=out_ref.at[tp],
+            dst_ref=back.at[tp],
             send_sem=tp_send.at[k],
             recv_sem=tp_recv.at[k],
             device_id=(sp, to),
@@ -237,71 +363,236 @@
         )
         copy.start()
         sends.append(copy)
-    out_ref[tp] = heads[tp]
-    for copy in started:
+    back[tp] = heads[tp]
+    for load in loads:
+        load.wait()
+    for k in (1, 2, 3):
+        source = (tp + 4 - k) % 4
+        pltpu.make_async_copy(back.at[source], back.at[source], tp_recv.at[k]).wait()
+
+    joined = jnp.concatenate(
+        [back[p, :, :128] for p in range(4)] + [back[p, :, 128:] for p in range(4)], axis=1
+    )
+
+    def project(n, total):
+        cols = pl.ds(pl.multiple_of(n * 256, 256), 256)
+        part = jnp.dot(joined, wo[:, cols], preferred_element_type=F32)
+        rounded = (resid_ref[:, cols].astype(F32) + part).astype(BF16)
+        middle[:, cols] = rounded
+        wide = rounded.astype(F32)
+        return total + jnp.sum(wide * wide, axis=1, keepdims=True)
+
+    total = lax.fori_loop(0, 8, project, jnp.zeros((64, 1), F32))
+    scale = lax.rsqrt(total / 2048.0 + EPSILON)
+    normed = (middle[...].astype(F32) * scale * norm_ref[...]).astype(BF16)
+    stack = jnp.concatenate([normed[:, j * 512 : j * 512 + 512] for j in range(4)], axis=0)
+
+    def device(o, other):
+        return (at(z + o[0], y + o[1], (core + other) % 2), (tp + o[2]) % 4)
+
+    def move(source, target, sem_out, sem_in, o, other):
+        pltpu.make_async_remote_copy(
+            src_ref=source,
+            dst_ref=target,
+            send_sem=sem_out,
+            recv_sem=sem_in,
+            device_id=device(o, other),
+            device_id_type=MESH,
+        ).start()
+
+    def to_relays(way, source, relay):
+        for g, (mask, lo, hi) in enumerate(GROUPS):
+            move(
+                source.at[pl.ds(lo, hi - lo)],
+                relay.at[pl.ds(lo, hi - lo)],
+                a2a_send.at[way * 4],
+                relay_recv.at[way * 8 + g],
+                [-v for v in mask],
+                0,
+            )
+
+    def from_relays(way, relay, target):
+        sign = 1 - 2 * way
+        for g, (mask, lo, hi) in enumerate(GROUPS):
+            there = relay.at[pl.ds(lo, hi - lo)]
+            pltpu.make_async_copy(there, there, relay_recv.at[way * 8 + g]).wait()
+            for k in range(lo, hi):
+                o = [sign * v + m for v, m in zip(ORDER[k][:3], mask)]
+                move(relay.at[k], target.at[k], a2a_send.at[way * 4 + 1], a2a_recv.at[way * 2], o, 1)
+
+    def direct(way, source, target, lo, hi):
+        sign = 1 - 2 * way
+        for k in range(lo, hi):
+            g = int(k >= 64)
+            move(
+                source.at[k],
+                target.at[k],
+                a2a_send.at[way * 4 + 2 + g],
+                a2a_recv.at[way * 2 + g],
+                [sign * v for v in ORDER[k][:3]],
+                ORDER[k][3],
+            )
+
+    def arrived(way, target, g):
+        part = target.at[pl.ds(g * 64, 64 - g)]
+        pltpu.make_async_copy(part, part, a2a_recv.at[way * 2 + g]).wait()
+
+    def fill_units(lo, hi):
+        for u in range(lo, hi):
+            rows_u = jnp.dot(fill[u * 256 : u * 256 + 256], stack, preferred_element_type=F32)
+            send[u * 16 : u * 16 + 16] = rows_u.astype(BF16).reshape(16, 16, 512)
+
+    fill_units(0, 4)
+    to_relays(0, send, relay_out)
+    direct(0, send, recv, RELAYED, 64)
+    fill_units(4, 8)
+    direct(0, send, recv, 64, FAR_END)
+    recv[127] = send[127]
+
+    def shared_hidden(n, carry):
+        cols = pl.ds(pl.multiple_of(n * 256, 256), 256)
+        gate = jnp.dot(normed, sg[:, cols], preferred_element_type=F32)
+        up = jnp.dot(normed, su[:, cols], preferred_element_type=F32)
+        hs[0:64, cols] = (gate * jax.nn.sigmoid(gate) * up).astype(BF16)
+        return carry
+
+    lax.fori_loop(0, 2, shared_hidden, 0)
+    from_relays(0, relay_out, recv)
+    direct(0, send, recv, FAR_END, 127)
+
+    def shared_down(n, carry):
+        cols = pl.ds(pl.multiple_of(n * 256, 256), 256)
+        shared[:, cols] = jnp.dot(hs[0:64, 0:512], sd[:, cols], preferred_element_type=F32)
+        return carry
+
+    lax.fori_loop(0, 8, shared_down, 0)
+
+    def expert(g):
+        for u in range(4):
+            s0 = (g * 4 + u) * 16
+            rows_u = jnp.dot(
+                perm[0], recv[s0 : s0 + 16].reshape(256, 512), preferred_element_type=F32
+            ).astype(BF16)
+            for j in range(4):
+                xs[u * 64 : u * 64 + 64, j * 512 : j * 512 + 512] = rows_u[j * 64 : j * 64 + 64]
+
+        def hidden(n, carry):
+            cols = pl.ds(pl.multiple_of(n * 256, 256), 256)
+            gate = jnp.dot(xs[...], wg[:, cols], preferred_element_type=F32)
+            up = jnp.dot(xs[...], wu[:, cols], preferred_element_type=F32)
+            hs[:, cols] = (gate * jax.nn.sigmoid(gate) * up).astype(BF16)
+            return carry
+
+        lax.fori_loop(0, 4, hidden, 0)
+
+        def down(n, carry):
+            cols = pl.ds(pl.multiple_of(n * 256, 256), 256)
+            rs[:, cols] = jnp.dot(hs[...], wd[:, cols], preferred_element_type=F32).astype(BF16)
+            return carry
+
+        lax.fori_loop(0, 8, down, 0)
+        for u in range(4):
+            s0 = (g * 4 + u) * 16
+            block = jnp.concatenate(
+                [rs[u * 64 : u * 64 + 64, j * 512 : j * 512 + 512] for j in range(4)], axis=0
+            )
+            rows_u = jnp.dot(perm[1], block, preferred_element_type=F32)
+            res[s0 : s0 + 16] = rows_u.astype(BF16).reshape(16, 16, 512)
+
+    arrived(0, recv, 0)
+    expert(0)
+    to_relays(1, res, relay_back)
+    direct(1, res, ret, RELAYED, 64)
+    arrived(0, recv, 1)
+    expert(1)
+    ret[127] = res[127]
+    direct(1, res, ret, 64, 127)
+    from_relays(1, relay_back, ret)
+
+    for g in range(2):
+        arrived(1, ret, g)
+        for half_cols in range(2):
+            cols = slice(half_cols * 256, half_cols * 256 + 256)
+            part = jnp.dot(
+                combine[:, g * 1024 : g * 1024 + 1024],
+                ret[g * 64 : g * 64 + 64].reshape(1024, 512)[:, cols],
+                preferred_element_type=F32,
+            )
+            if g == 0:
+                routed[:, cols] = part
+            else:
+                routed[:, cols] = routed[:, cols] + part
+    for j in range(4):
+        cols = slice(j * 512, j * 512 + 512)
+        rows_j = routed[j * 64 : j * 64 + 64] + routed[256 + j * 64 : 256 + j * 64 + 64]
+        out_ref[:, cols] = (middle[:, cols].astype(F32) + shared[:, cols] + rows_j).astype(BF16)
+
+    for copy in started + sends:
         copy.wait_send()
-    for k in (1, 2, 3):
-        sends[k - 1].wait_send()
-        source = (tp + 4 - k) % 4
-        pltpu.make_async_copy(out_ref.at[source], out_ref.at[source], tp_recv.at[k]).wait()
-
-
-def attention(q, piece, lam, gain):
+    for way, (buffer, relay) in enumerate(((send, relay_out), (res, relay_back))):
+        for k, part in enumerate(
+            (
+                relay.at[pl.ds(0, RELAYED)],
+                relay.at[pl.ds(0, RELAYED)],
+                buffer.at[pl.ds(RELAYED, 64 - RELAYED)],
+                buffer.at[pl.ds(64, 63)],
+            )
+        ):
+            pltpu.make_async_copy(part, part, a2a_send.at[way * 4 + k]).wait()
+
+
+def layer(q, piece, lam, gain, resid, norm, ids, mix, weights):
     rows = q.shape[0]
+    tokens, width = resid.shape
+    table = np.zeros((8, 2048), np.int32)
+    table[:4] = np.repeat(np.array(ORDER, np.int32).T, 16, axis=1)
+    vmem = pl.BlockSpec(memory_space=pltpu.VMEM)
+    smem = pl.BlockSpec(memory_space=pltpu.SMEM)
+    slots = pltpu.VMEM((128, 16, 512), BF16)
+    relays = pltpu.VMEM((RELAYED, 16, 512), BF16)
     return pl.pallas_call(
-        attention_kernel,
-        out_shape=jax.ShapeDtypeStruct((4, rows // 4, 256), BF16),
-        in_specs=[
-            pl.BlockSpec(memory_space=pltpu.VMEM),
-            pl.BlockSpec(memory_space=pltpu.VMEM),
-            pl.BlockSpec(memory_space=pltpu.SMEM),
-            pl.BlockSpec(memory_space=pltpu.VMEM),
-        ],
-        out_specs=pl.BlockSpec(memory_space=pltpu.VMEM),
+        layer_kernel,
+        out_shape=jax.ShapeDtypeStruct((tokens, width), BF16),
+        in_specs=[vmem, vmem, smem] + [vmem] * 6 + [pl.BlockSpec(memory_space=pl.ANY)] * 7,
+        out_specs=vmem,
         scratch_shapes=[
             pltpu.VMEM((32, rows, 640), BF16),
             pltpu.VMEM((4, rows // 4, 256), BF16),
+            pltpu.VMEM((4, rows // 4, 256), BF16),
             pltpu.VMEM((4, 136, rows), F32),
             pltpu.VMEM((8, rows), F32),
+        ]
+        + [pltpu.VMEM(weights[k].shape, BF16) for k in (0, 1, 2, 3, 4, 5, 6)]
+        + [
+            pltpu.VMEM((2048, 256), BF16),
+            pltpu.VMEM((512, 2048), BF16),
+            pltpu.VMEM((2, 256, 256), BF16),
+            pltpu.VMEM((tokens, width), BF16),
+            pltpu.VMEM((tokens, width), F32),
+            slots,
+            slots,
+            slots,
+            slots,
+            relays,
+            relays,
+            pltpu.VMEM((256, width), BF16),
+            pltpu.VMEM((256, 1024), BF16),
+            pltpu.VMEM((256, width), BF16),
+            pltpu.VMEM((512, 512), F32),
             pltpu.SemaphoreType.DMA((64,)),
             pltpu.SemaphoreType.DMA((32,)),
             pltpu.SemaphoreType.DMA((16,)),
             pltpu.SemaphoreType.DMA((4,)),
             pltpu.SemaphoreType.DMA((4,)),
+            pltpu.SemaphoreType.DMA((7,)),
+            pltpu.SemaphoreType.DMA((8,)),
+            pltpu.SemaphoreType.DMA((4,)),
+            pltpu.SemaphoreType.DMA((16,)),
         ],
         compiler_params=pltpu.CompilerParams(
-            vmem_limit_bytes=48 * 1024 * 1024, collective_id=0, has_side_effects=True
+            vmem_limit_bytes=63 * 1024 * 1024, collective_id=0, has_side_effects=True
         ),
-    )(q, piece, lam, gain)
-
-
-def swiglu_rows(row_set, w_gate, w_up, w_down):
-    gate_val = jnp.dot(row_set, w_gate, preferred_element_type=F32)
-    up_val = jnp.dot(row_set, w_up, preferred_element_type=F32)
-    hidden = (jax.nn.silu(gate_val) * up_val).astype(BF16)
-    return jnp.dot(hidden, w_down, preferred_element_type=F32)
-
-
-def slot_matrices(expert_ids, expert_mix, experts, capacity):
-    tokens, top_count = expert_ids.shape
-    named = jnp.sum(
-        (expert_ids[:, :, None] == jnp.arange(experts, dtype=jnp.int32)).astype(F32), axis=1
-    )
-    mix = jnp.sum(
-        jnp.where(
-            expert_ids[:, :, None] == jnp.arange(experts, dtype=jnp.int32),
-            expert_mix[:, :, None],
-            0.0,
-        ),
-        axis=1,
-    )
-    before = jnp.tril(jnp.ones((tokens, tokens), F32), -1)
-    rank = jnp.dot(before, named, preferred_element_type=F32)
-    slot = jnp.arange(capacity, dtype=F32)
-    hit = (rank[:, :, None] == slot) & (named[:, :, None] > 0)
-    fill = hit.astype(BF16).reshape(tokens, experts * capacity)
-    weight = jnp.where(hit, mix[:, :, None], 0.0).reshape(tokens, experts * capacity)
-    return fill, weight
+    )(q, piece, lam, gain, resid, norm, ids, mix, jnp.asarray(table), *weights)
 
 
 def per_device(
@@ -327,11 +618,6 @@
     shared_down,
 ):
     rows = query_a.shape[0]
-    sp_count = lax.axis_size("sp")
-    tp_count = lax.axis_size("tp")
-    experts = sp_count * tp_count
-    tok_dev, width = resid.shape
-    capacity = 4
     qa = query_a[:, 0]
     zero = jnp.zeros((rows, 64), BF16)
     q = jnp.concatenate([qa[:, :64], zero, zero, qa[:, 64:], query_b[:, 0]], axis=1)
@@ -344,30 +630,26 @@
         axis=1,
     )
     lam = jnp.concatenate([lambda_a, lambda_b])
-    back = attention(q, piece, lam, head_gain[None, :])
-    joined = jnp.concatenate(
-        [back[:, :, :128].transpose(1, 0, 2).reshape(tok_dev, -1),
-         back[:, :, 128:].transpose(1, 0, 2).reshape(tok_dev, -1)], axis=1)
-    project = jnp.dot(joined, out_weight, preferred_element_type=F32)
-    middle = (resid.astype(F32) + project).astype(BF16)
-    middle_f = middle.astype(F32)
-    normed = (
-        middle_f
-        * lax.rsqrt(jnp.mean(middle_f * middle_f, axis=1, keepdims=True) + EPSILON)
-        * norm_gain[None, :]
-    ).astype(BF16)
-    shared = swiglu_rows(normed, shared_gate, shared_up, shared_down)
-    fill, weight = slot_matrices(expert_ids, expert_mix, experts, capacity)
-    send = jnp.dot(fill.T, normed, preferred_element_type=F32).astype(BF16)
-    arrived = lax.all_to_all(send, ("sp", "tp"), split_axis=0, concat_axis=0, tiled=True)
-    result = swiglu_rows(arrived, gate_experts[0], up_experts[0], down_experts[0]).astype(BF16)
-    returned = lax.all_to_all(result, ("sp", "tp"), split_axis=0, concat_axis=0, tiled=True)
-    high = weight.astype(BF16)
-    low = (weight - high.astype(F32)).astype(BF16)
-    routed = jnp.dot(high, returned, preferred_element_type=F32) + jnp.dot(
-        low, returned, preferred_element_type=F32
+    weights = (
+        out_weight,
+        gate_experts[0],
+        up_experts[0],
+        down_experts[0],
+        shared_gate,
+        shared_up,
+        shared_down,
     )
-    return (middle_f + shared + routed).astype(BF16)
+    return layer(
+        q,
+        piece,
+        lam,
+        head_gain[None, :],
+        resid,
+        norm_gain[None, :],
+        expert_ids,
+        expert_mix,
+        weights,
+    )
 
 
 def solution(mesh):

time: 181 us -> 145 us (0.80)
  Pallas kernels: 42.8 us -> 132 us
  blocking collectives: 48.5 us -> 0 us
  matrix products: 35.8 us -> 0 us
  waiting for transfers between devices: 28.4 us -> 0 us
  local copies, waits for them, and re-layouts: 16.4 us -> 7.39 us
  starting transfers between devices: 4.84 us -> 0 us
  other arithmetic: 2.19 us -> 4.02 us
    pallas_call x1, Pallas kernels: 42.8 us -> 132 us  [layer(): pl.pallas_call(layer_kernel, out_shape=jax.ShapeDtypeStruct((tokens, widt...]
    all_to_all x1 -> x0, blocking collectives: 48.5 us -> none  [per_device(): lax.all_to_all(send, ('sp', 'tp'), split_axis=0, concat_axis=0, tiled=True)]
    dot_general x9 -> x0, matrix products: 35.8 us -> none  [the longest x2 13.8 us: swiglu_rows(): return jnp.dot(hidden, w_down, preferred_element_type=F32)]
    all_to_all x1 -> x0, waiting for transfers between devices: 28.4 us -> none  [per_device(): lax.all_to_all(result, ('sp', 'tp'), split_axis=0, concat_axis=0, tiled=T...]
    all_to_all x3 -> x0, local copies, waits for them, and re-layouts: 12.1 us -> none  [the longest x2 8.03 us: per_device(): lax.all_to_all(send, ('sp', 'tp'), split_axis=0, concat_axis=0, tiled=True)]
    all_to_all x1 -> x0, starting transfers between devices: 4.84 us -> none  [per_device(): lax.all_to_all(result, ('sp', 'tp'), split_axis=0, concat_axis=0, tiled=T...]
    unnamed x17 -> x5, local copies, waits for them, and re-layouts: 2.8 us -> 6.31 us
  transfers between devices with their start and end apart: 1 -> 0, of which waited for: 1 -> 0; matrix products, arithmetic and copies ran while one was open for 1% -> 0% of each run, Pallas kernels for 0% -> 0%
where the time goes in v3:
time: 145 us
  Pallas kernels  132 us (91%)
  local copies, waits for them, and re-layouts  7.39 us (5%)
  other arithmetic  4.02 us (3%)
    pallas_call x1, Pallas kernels, layer(): pl.pallas_call(layer_kernel, out_shape=jax.ShapeDtypeStruct((tokens, widt...  132 us
    unnamed x5, local copies, waits for them, and re-layouts  6.31 us

profile of v3, /device:TPU:1, one launch (start us, length us, event | category | flops | bytes accessed | tf_op | source)
XLA Modules:
  0.0 145.0 jit_solution(17671613778373779532)
XLA Ops:
  1.3 0.6 pad_maximum_fusion.1.lam_ref
  1.9 0.1 pad.7.clone
  2.0 1.4 copy.24.ids_ref
  3.4 1.4 copy.25.mix_ref
  4.8 0.9 copy.22
  5.7 0.9 copy.23
  6.7 1.0 fusion
  7.7 1.7 %pad_maximum_fusion.q_ref = bf16[256,512]{1,0:T(8,128)(2,1)} fusion(bf16[256,256]{1,0:T(8,128)(2,1)} %bitcast.22, bf16[256,64]{1,0:T(8,128)(2,1)S(1)} %get-tuple-element.6, bf16[256,64]{1,0:T(8,128)(2,1)S(1)} %get-tuple-element.5, bf16[512]{0:T(512)(128)(2,1)S(1)} %pad.7.clone), kind=kLoop, calls=%fused_computation.1 | loop fusion | flops 1048576 | bytes 459776 | tf_op jit(solution)/shard_map/concatenate | solution.py:623
  9.4 1.7 %maximum_maximum_fusion.own_ref = bf16[256,640]{1,0:T(8,128)(2,1)} fusion(bf16[128,256]{1,0:T(8,128)(2,1)S(1)} %bitcast.19, bf16[128,256]{1,0:T(8,128)(2,1)S(1)} %bitcast.18, bf16[256,256]{1,0:T(8,128)(2,1)} %bitcast.21, bf16[256,128]{1,0:T(8,128)(2,1)} %bitcast.23), kind=kLoop, calls=%fused_computation | loop fusion | flops 1310720 | bytes 655360 | tf_op jit(solution)/shard_map/concatenate | solution.py:624
  11.1 132.3 %shard_map.199 = bf16[64,2048]{1,0:T(8,128)(2,1)} custom-call(bf16[256,512]{1,0:T(8,128)(2,1)} %pad_maximum_fusion.q_ref, bf16[256,640]{1,0:T(8,128)(2,1)} %maximum_maximum_fusion.own_ref, f32[2]{0:T(128)} %pad_maximum_fusion.1.lam_ref, f32[1,128]{1,0:T(1,128)} %bitcast.25, bf16[64,2048]{1,0:T(8,128)(2,1)} %resid_ref.1, f32[1,2048]{1,0:T(1,128)} %bitcast.24, ...), custom_call_target="tpu_custom_call" | custom-call | tf_op jit(solution)/shard_map/pallas_call | solution.py:553
  143.4 1.7 %copy.29 = bf16[64,2048]{1,0:T(8,128)(2,1)} copy(bf16[64,2048]{1,0:T(8,128)(2,1)} %shard_map.199) | data formatting | bytes 524288
  (1 shorter events, 0.0 us)

commit v4 on v3

--- a/solution.py
+++ b/solution.py
@@ -16,39 +16,28 @@
 F32 = jnp.float32
 
 
-def dot_nt(a, b):
-    return lax.dot_general(a, b, (((1,), (1,)), ((), ())), preferred_element_type=F32)
-
-
 MESH = pl.DeviceIdType.MESH
 SIDE = 4
 
 
 def flows():
     every = [(a, b, c) for a in range(SIDE) for b in range(SIDE) for c in range(SIDE)]
-    order, groups = [], []
-    for mask in itertools.product((0, 1), repeat=3):
-        if any(mask):
-            members = [o for o in every if tuple(int(v == 2) for v in o) == mask]
-            groups.append((mask, len(order), len(order) + len(members)))
-            order += [o + (1,) for o in members]
-    far = [o for o in every if 2 in o]
-    near = [o for o in every if 2 not in o]
-    order += [o + (1,) for o in near]
-    order += [o + (0,) for o in far]
-    order += [o + (0,) for o in near if any(o)] + [(0, 0, 0, 0)]
-    return order, groups
-
-
-ORDER, GROUPS = flows()
-RELAYED = GROUPS[-1][2]
-FAR_END = 64 + RELAYED
+    order = [o + (1,) for o in every] + [o + (0,) for o in every if any(o)]
+    return order + [(0, 0, 0, 0)]
+
+
+ORDER = flows()
 
 
 def layer_kernel(
-    q_ref,
-    own_ref,
-    lam_ref,
+    qa_ref,
+    ka_ref,
+    va_ref,
+    qb_ref,
+    kb_ref,
+    vb_ref,
+    la_ref,
+    lb_ref,
     gain_ref,
     resid_ref,
     norm_ref,
@@ -63,6 +52,7 @@
     su_hbm,
     sd_hbm,
     out_ref,
+    qt,
     kv,
     heads,
     back,
@@ -84,8 +74,6 @@
     recv,
     res,
     ret,
-    relay_out,
-    relay_back,
     xs,
     hs,
     rs,
@@ -98,7 +86,6 @@
     load_sem,
     a2a_send,
     a2a_recv,
-    relay_recv,
 ):
     sp = lax.axis_index("sp")
     tp = lax.axis_index("tp")
@@ -106,7 +93,7 @@
     chip = sp // 2
     z = chip // SIDE
     y = chip % SIDE
-    rows = q_ref.shape[0]
+    rows = qa_ref.shape[0]
     half = rows // 2
     ones = jnp.ones((8, 2 * rows), BF16)
     scale_a = LOG2E * 64**-0.5
@@ -138,6 +125,17 @@
         return carry
 
     lax.fori_loop(1, 128, greet, 0)
+
+    turned = qa_ref[...].astype(F32).T.astype(BF16)
+    nothing = jnp.zeros((64, rows), BF16)
+    qt[0] = jnp.concatenate([turned[:64], nothing], axis=0)
+    qt[1] = jnp.concatenate([nothing, turned[64:]], axis=0)
+    qt[2] = qb_ref[:, :128].astype(F32).T.astype(BF16)
+    qt[3] = qb_ref[:, 128:].astype(F32).T.astype(BF16)
+    kv[sp, :, 0:128] = ka_ref[...]
+    kv[sp, :, 128:384] = kb_ref[...]
+    kv[sp, 0:128, 384:640] = va_ref[...].astype(F32).T.astype(BF16)
+    kv[sp, 128:256, 384:640] = vb_ref[...].astype(F32).T.astype(BF16)
     pl.semaphore_wait(barrier, 127)
 
     started = []
@@ -154,10 +152,8 @@
         new[along] = (new[along] + step) % SIDE
         lo, size = (h * half, half) if part is None else (h * half + part * half // 2, half // 2)
         p = piece_of(h, o1, o2)
-        own = o1 == 0 and o2 == 0
-        source = own_ref.at[pl.ds(lo, size)] if own else kv.at[p, pl.ds(lo, size)]
         copy = pltpu.make_async_remote_copy(
-            src_ref=source,
+            src_ref=kv.at[p, pl.ds(lo, size)],
             dst_ref=kv.at[p, pl.ds(lo, size)],
             send_sem=send_sem.at[len(started)],
             recv_sem=half_sem.at[h * 16 + new[0] * 4 + new[1]],
@@ -194,7 +190,7 @@
     def pair_send(a, b):
         p = at(z - a, y - b, core)
         copy = pltpu.make_async_remote_copy(
-            src_ref=own_ref if (a, b) == (0, 0) else kv.at[p],
+            src_ref=kv.at[p],
             dst_ref=kv.at[p],
             send_sem=send_sem.at[len(started)],
             recv_sem=pair_sem.at[a * 4 + b],
@@ -219,7 +215,7 @@
                 h = head * 2 + m
                 lo = [0, 0, 128, 256][h]
                 keys = jnp.concatenate([p[:, lo : lo + 128] for p in piece], axis=0)
-                s = dot_nt(keys, q_ref[:, h * 128 : h * 128 + 128])
+                s = jnp.dot(keys, qt[h], preferred_element_type=F32)
                 s = s * (scale_a if head == 0 else scale_b)
                 if masked:
                     s = jnp.where(keep, s, NEG)
@@ -263,15 +259,17 @@
         expert = at(z + oz, y + oy, (core + oc) % 2) * 4 + (tp + ox) % 4
         named = jnp.zeros((64, 2048), F32)
         mixed = jnp.zeros((64, 2048), F32)
+        down = lax.broadcasted_iota(jnp.int32, (64, 64), 0)
+        across = lax.broadcasted_iota(jnp.int32, (64, 64), 1)
+
+        def column(row):
+            return jnp.sum(jnp.where(down == across, row, jnp.zeros_like(row)), axis=1, keepdims=True)
+
         for k in range(4):
-            same = ids_ref[:, k : k + 1] == expert
+            same = column(ids_ref[k : k + 1, :]) == expert
             named = named + jnp.where(same, 1.0, 0.0)
-            mixed = mixed + jnp.where(same, mix_ref[:, k : k + 1], 0.0)
-        before = jnp.where(
-            lax.broadcasted_iota(jnp.int32, (64, 64), 1) < lax.broadcasted_iota(jnp.int32, (64, 64), 0),
-            1.0,
-            0.0,
-        ).astype(BF16)
+            mixed = mixed + jnp.where(same, column(mix_ref[k : k + 1, :]), 0.0)
+        before = jnp.where(across < down, 1.0, 0.0).astype(BF16)
         rank = jnp.dot(before, named.astype(BF16), preferred_element_type=F32)
         hit = (named > 0.5) & (jnp.abs(rank - (lane % 4).astype(F32)) < 0.5)
         placed = jnp.where(hit, 1.0, 0.0)
@@ -298,7 +296,6 @@
     pair_send(0, 0)
     for h in range(2):
         spread(h, 0, 0, 1)
-    kv[sp] = own_ref[...]
     pltpu.make_async_copy(kv.at[sp], kv.at[sp], pair_sem.at[0]).wait()
     chunk(chip, True, True)
 
@@ -346,7 +343,7 @@
         second = acc[2 * head + 1]
         one = first[0:128] / first[128:129]
         two = second[0:128] / second[128:129]
-        differ = one - lam_ref[head] * two
+        differ = one - (la_ref, lb_ref)[head][...] * two
         scale = lax.rsqrt(jnp.mean(differ * differ, axis=0, keepdims=True) + EPSILON)
         done = (differ * scale).T * gain_ref[...] * HEAD_SCALE
         heads[:, :, head * 128 : head * 128 + 128] = done.astype(BF16).reshape(4, rows // 4, 128)
@@ -400,26 +397,6 @@
             device_id_type=MESH,
         ).start()
 
-    def to_relays(way, source, relay):
-        for g, (mask, lo, hi) in enumerate(GROUPS):
-            move(
-                source.at[pl.ds(lo, hi - lo)],
-                relay.at[pl.ds(lo, hi - lo)],
-                a2a_send.at[way * 4],
-                relay_recv.at[way * 8 + g],
-                [-v for v in mask],
-                0,
-            )
-
-    def from_relays(way, relay, target):
-        sign = 1 - 2 * way
-        for g, (mask, lo, hi) in enumerate(GROUPS):
-            there = relay.at[pl.ds(lo, hi - lo)]
-            pltpu.make_async_copy(there, there, relay_recv.at[way * 8 + g]).wait()
-            for k in range(lo, hi):
-                o = [sign * v + m for v, m in zip(ORDER[k][:3], mask)]
-                move(relay.at[k], target.at[k], a2a_send.at[way * 4 + 1], a2a_recv.at[way * 2], o, 1)
-
     def direct(way, source, target, lo, hi):
         sign = 1 - 2 * way
         for k in range(lo, hi):
@@ -427,7 +404,7 @@
             move(
                 source.at[k],
                 target.at[k],
-                a2a_send.at[way * 4 + 2 + g],
+                a2a_send.at[way * 2 + g],
                 a2a_recv.at[way * 2 + g],
                 [sign * v for v in ORDER[k][:3]],
                 ORDER[k][3],
@@ -442,11 +419,11 @@
             rows_u = jnp.dot(fill[u * 256 : u * 256 + 256], stack, preferred_element_type=F32)
             send[u * 16 : u * 16 + 16] = rows_u.astype(BF16).reshape(16, 16, 512)
 
-    fill_units(0, 4)
-    to_relays(0, send, relay_out)
-    direct(0, send, recv, RELAYED, 64)
-    fill_units(4, 8)
-    direct(0, send, recv, 64, FAR_END)
+    for u in range(8):
+        fill_units(u, u + 1)
+        if u > 0:
+            direct(0, send, recv, u * 16 - 16, u * 16)
+    direct(0, send, recv, 112, 127)
     recv[127] = send[127]
 
     def shared_hidden(n, carry):
@@ -457,8 +434,6 @@
         return carry
 
     lax.fori_loop(0, 2, shared_hidden, 0)
-    from_relays(0, relay_out, recv)
-    direct(0, send, recv, FAR_END, 127)
 
     def shared_down(n, carry):
         cols = pl.ds(pl.multiple_of(n * 256, 256), 256)
@@ -501,13 +476,11 @@
 
     arrived(0, recv, 0)
     expert(0)
-    to_relays(1, res, relay_back)
-    direct(1, res, ret, RELAYED, 64)
+    direct(1, res, ret, 0, 64)
     arrived(0, recv, 1)
     expert(1)
     ret[127] = res[127]
     direct(1, res, ret, 64, 127)
-    from_relays(1, relay_back, ret)
 
     for g in range(2):
         arrived(1, ret, g)
@@ -529,33 +502,26 @@
 
     for copy in started + sends:
         copy.wait_send()
-    for way, (buffer, relay) in enumerate(((send, relay_out), (res, relay_back))):
-        for k, part in enumerate(
-            (
-                relay.at[pl.ds(0, RELAYED)],
-                relay.at[pl.ds(0, RELAYED)],
-                buffer.at[pl.ds(RELAYED, 64 - RELAYED)],
-                buffer.at[pl.ds(64, 63)],
-            )
-        ):
-            pltpu.make_async_copy(part, part, a2a_send.at[way * 4 + k]).wait()
-
-
-def layer(q, piece, lam, gain, resid, norm, ids, mix, weights):
-    rows = q.shape[0]
+    for way, buffer in enumerate((send, res)):
+        for g in range(2):
+            part = buffer.at[pl.ds(g * 64, 64 - g)]
+            pltpu.make_async_copy(part, part, a2a_send.at[way * 2 + g]).wait()
+
+
+def layer(qkv, lambdas, gain, resid, norm, ids, mix, weights):
+    rows = qkv[0].shape[0]
     tokens, width = resid.shape
     table = np.zeros((8, 2048), np.int32)
     table[:4] = np.repeat(np.array(ORDER, np.int32).T, 16, axis=1)
     vmem = pl.BlockSpec(memory_space=pltpu.VMEM)
-    smem = pl.BlockSpec(memory_space=pltpu.SMEM)
     slots = pltpu.VMEM((128, 16, 512), BF16)
-    relays = pltpu.VMEM((RELAYED, 16, 512), BF16)
     return pl.pallas_call(
         layer_kernel,
         out_shape=jax.ShapeDtypeStruct((tokens, width), BF16),
-        in_specs=[vmem, vmem, smem] + [vmem] * 6 + [pl.BlockSpec(memory_space=pl.ANY)] * 7,
+        in_specs=[vmem] * 14 + [pl.BlockSpec(memory_space=pl.ANY)] * 7,
         out_specs=vmem,
         scratch_shapes=[
+            pltpu.VMEM((4, 128, rows), BF16),
             pltpu.VMEM((32, rows, 640), BF16),
             pltpu.VMEM((4, rows // 4, 256), BF16),
             pltpu.VMEM((4, rows // 4, 256), BF16),
@@ -573,8 +539,6 @@
             slots,
             slots,
             slots,
-            relays,
-            relays,
             pltpu.VMEM((256, width), BF16),
             pltpu.VMEM((256, 1024), BF16),
             pltpu.VMEM((256, width), BF16),
@@ -585,14 +549,13 @@
             pltpu.SemaphoreType.DMA((4,)),
             pltpu.SemaphoreType.DMA((4,)),
             pltpu.SemaphoreType.DMA((7,)),
-            pltpu.SemaphoreType.DMA((8,)),
             pltpu.SemaphoreType.DMA((4,)),
-            pltpu.SemaphoreType.DMA((16,)),
+            pltpu.SemaphoreType.DMA((4,)),
         ],
         compiler_params=pltpu.CompilerParams(
             vmem_limit_bytes=63 * 1024 * 1024, collective_id=0, has_side_effects=True
         ),
-    )(q, piece, lam, gain, resid, norm, ids, mix, jnp.asarray(table), *weights)
+    )(*qkv, *lambdas, gain, resid, norm, ids, mix, jnp.asarray(table), *weights)
 
 
 def per_device(
@@ -617,19 +580,6 @@
     shared_up,
     shared_down,
 ):
-    rows = query_a.shape[0]
-    qa = query_a[:, 0]
-    zero = jnp.zeros((rows, 64), BF16)
-    q = jnp.concatenate([qa[:, :64], zero, zero, qa[:, 64:], query_b[:, 0]], axis=1)
-    piece = jnp.concatenate(
-        [
-            key_a[:, 0],
-            key_b[:, 0],
-            jnp.concatenate([value_a[:, 0].T, value_b[:, 0].T], axis=0),
-        ],
-        axis=1,
-    )
-    lam = jnp.concatenate([lambda_a, lambda_b])
     weights = (
         out_weight,
         gate_experts[0],
@@ -639,15 +589,15 @@
         shared_up,
         shared_down,
     )
+    qkv = [a[:, 0] for a in (query_a, key_a, value_a, query_b, key_b, value_b)]
     return layer(
-        q,
-        piece,
-        lam,
+        qkv,
+        (lambda_a[None, :], lambda_b[None, :]),
         head_gain[None, :],
         resid,
         norm_gain[None, :],
-        expert_ids,
-        expert_mix,
+        expert_ids.T,
+        expert_mix.T,
         weights,
     )
 

time: 145 us -> 137 us (0.945)
  the two profiles are of different devices: /device:TPU:1 before, /device:TPU:11 now
where the time goes in v4:
time: 137 us
  Pallas kernels  134 us (98%)
  local copies, waits for them, and re-layouts  1.67 us (1%)
    pallas_call x1, Pallas kernels, layer(): pl.pallas_call(layer_kernel, out_shape=jax.ShapeDtypeStruct((tokens, widt...  134 us

profile of v4, /device:TPU:11, one launch (start us, length us, event | category | flops | bytes accessed | tf_op | source)
XLA Modules:
  0.0 136.7 jit_solution(15068007850837606787)
XLA Ops:
  1.3 133.7 %shard_map.199 = bf16[64,2048]{1,0:T(8,128)(2,1)} custom-call(bf16[256,128]{1,0:T(8,128)(2,1)} %bitcast.22, bf16[256,128]{1,0:T(8,128)(2,1)} %bitcast.23, bf16[256,128]{1,0:T(8,128)(2,1)} %bitcast.24, bf16[256,256]{1,0:T(8,128)(2,1)} %bitcast.20, bf16[256,256]{1,0:T(8,128)(2,1)} %bitcast.21, bf16[256,128]{1,0:T(8,128)(2,1)} %bitcast.25, ...), custom_call_target="tpu_custom_call" | custom-call | tf_op jit(solution)/shard_map/pallas_call | solution.py:518
  135.0 1.7 %copy.25 = bf16[64,2048]{1,0:T(8,128)(2,1)} copy(bf16[64,2048]{1,0:T(8,128)(2,1)} %shard_map.199) | data formatting | bytes 524288

commit v5 on v4

--- a/solution.py
+++ b/solution.py
@@ -10,7 +10,6 @@
 
 EPSILON = 1e-05
 HEAD_SCALE = 0.8
-LOG2E = 1.4426950408889634
 NEG = -1e30
 BF16 = jnp.bfloat16
 F32 = jnp.float32
@@ -21,9 +20,13 @@
 
 
 def flows():
-    every = [(a, b, c) for a in range(SIDE) for b in range(SIDE) for c in range(SIDE)]
-    order = [o + (1,) for o in every] + [o + (0,) for o in every if any(o)]
-    return order + [(0, 0, 0, 0)]
+    every = np.array([o for o in itertools.product(range(SIDE), range(SIDE), range(SIDE), (0, 1)) if any(o)])
+    mixed = every[np.random.RandomState(1).permutation(len(every))]
+    hops = np.minimum(mixed[:, :3], SIDE - mixed[:, :3]).sum(axis=1)
+    mixed = mixed[np.argsort(-hops, kind="stable")]
+    for part in (mixed[:64], mixed[64:]):
+        part[:] = part[np.random.RandomState(2).permutation(len(part))]
+    return [tuple(int(v) for v in o) for o in mixed] + [(0, 0, 0, 0)]
 
 
 ORDER = flows()
@@ -96,8 +99,6 @@
     rows = qa_ref.shape[0]
     half = rows // 2
     ones = jnp.ones((8, 2 * rows), BF16)
-    scale_a = LOG2E * 64**-0.5
-    scale_b = LOG2E * 128**-0.5
 
     def at(zz, yy, cc):
         return ((zz % SIDE) * SIDE + yy % SIDE) * 2 + cc
@@ -206,30 +207,42 @@
             key_pos = lax.broadcasted_iota(jnp.int32, (2 * rows, rows), 0)
             query_pos = lax.broadcasted_iota(jnp.int32, (2 * rows, rows), 1) + core * rows
             keep = key_pos <= query_pos
-        for head in range(2):
-            vt = jnp.concatenate(
-                [p[head * 128 : head * 128 + 128, 384:640] for p in piece], axis=1
+        values = [
+            jnp.concatenate(
+                [
+                    jnp.concatenate(
+                        [p[head * 128 : head * 128 + 128, 384:640] for p in piece], axis=1
+                    ),
+                    ones,
+                ],
+                axis=0,
             )
-            vt = jnp.concatenate([vt, ones], axis=0)
-            for m in range(2):
-                h = head * 2 + m
-                lo = [0, 0, 128, 256][h]
-                keys = jnp.concatenate([p[:, lo : lo + 128] for p in piece], axis=0)
-                s = jnp.dot(keys, qt[h], preferred_element_type=F32)
-                s = s * (scale_a if head == 0 else scale_b)
-                if masked:
-                    s = jnp.where(keep, s, NEG)
-                best = jnp.max(s, axis=0, keepdims=True)
-                if not first:
-                    old = top[h : h + 1, :]
-                    best = jnp.maximum(best, old)
-                p = jnp.exp2(s - best).astype(BF16)
-                add = jnp.dot(vt, p, preferred_element_type=F32)
-                if first:
-                    acc[h] = add
-                else:
-                    acc[h] = acc[h] * jnp.exp2(old - best) + add
-                top[h : h + 1, :] = best
+            for head in range(2)
+        ]
+
+        def scores(h):
+            lo = (0, 0, 128, 256)[h]
+            keys = jnp.concatenate([p[:, lo : lo + 128] for p in piece], axis=0)
+            s = jnp.dot(keys, qt[h], preferred_element_type=F32)
+            return jnp.where(keep, s, NEG) if masked else s
+
+        ready = scores(0)
+        for h in range(4):
+            s = ready
+            if h < 3:
+                ready = scores(h + 1)
+            scale = (64**-0.5, 64**-0.5, 128**-0.5, 128**-0.5)[h]
+            best = jnp.max(s, axis=0, keepdims=True)
+            if not first:
+                old = top[h : h + 1, :]
+                best = jnp.maximum(best, old)
+            p = jnp.exp((s - best) * scale).astype(BF16)
+            add = jnp.dot(values[h // 2], p, preferred_element_type=F32)
+            if first:
+                acc[h] = add
+            else:
+                acc[h] = acc[h] * jnp.exp((old - best) * scale) + add
+            top[h : h + 1, :] = best
 
     def chunks(offsets):
         code = 0

time: 137 us -> 113 us (0.82)
  the two profiles are of different devices: /device:TPU:11 before, /device:TPU:1 now
where the time goes in v5:
time: 113 us
  Pallas kernels  110 us (97%)
  local copies, waits for them, and re-layouts  1.67 us (1%)
  between operations  1.3 us (1%)
    pallas_call x1, Pallas kernels, layer(): pl.pallas_call(layer_kernel, out_shape=jax.ShapeDtypeStruct((tokens, widt...  110 us

profile of v5, /device:TPU:1, one launch (start us, length us, event | category | flops | bytes accessed | tf_op | source)
XLA Modules:
  0.0 112.9 jit_solution(1904542924254202141)
XLA Ops:
  1.3 110.0 %shard_map.199 = bf16[64,2048]{1,0:T(8,128)(2,1)} custom-call(bf16[256,128]{1,0:T(8,128)(2,1)} %bitcast.22, bf16[256,128]{1,0:T(8,128)(2,1)} %bitcast.23, bf16[256,128]{1,0:T(8,128)(2,1)} %bitcast.24, bf16[256,256]{1,0:T(8,128)(2,1)} %bitcast.20, bf16[256,256]{1,0:T(8,128)(2,1)} %bitcast.21, bf16[256,128]{1,0:T(8,128)(2,1)} %bitcast.25, ...), custom_call_target="tpu_custom_call" | custom-call | tf_op jit(solution)/shard_map/pallas_call | solution.py:531
  111.3 1.7 %copy.25 = bf16[64,2048]{1,0:T(8,128)(2,1)} copy(bf16[64,2048]{1,0:T(8,128)(2,1)} %shard_map.199) | data formatting | bytes 524288

commit v6 on v5

--- a/solution.py
+++ b/solution.py
@@ -100,13 +100,21 @@
     half = rows // 2
     ones = jnp.ones((8, 2 * rows), BF16)
 
-    def at(zz, yy, cc):
-        return ((zz % SIDE) * SIDE + yy % SIDE) * 2 + cc
+    z_at = [lax.rem(z + k, SIDE) * (SIDE * 2) for k in range(SIDE)]
+    y_at = [lax.rem(y + k, SIDE) * 2 for k in range(SIDE)]
+    core_at = [core, 1 - core]
+    tp_at = [lax.rem(tp + k, SIDE) for k in range(SIDE)]
+
+    def at(dz, dy, other):
+        return z_at[dz % SIDE] + y_at[dy % SIDE] + core_at[other]
+
+    def device(o, other):
+        return (at(o[0], o[1], other), tp_at[o[2] % SIDE])
 
     def neighbour(dim, step):
-        return (at(z + step, y, core), tp) if dim == 0 else (at(z, y + step, core), tp)
-
-    partner = (at(z, y, 1 - core), tp)
+        return (at(step, 0, 0), tp) if dim == 0 else (at(0, step, 0), tp)
+
+    partner = (at(0, 0, 1), tp)
     loads = [
         pltpu.make_async_copy(source, target, load_sem.at[k])
         for k, (source, target) in enumerate(
@@ -115,17 +123,11 @@
     ]
     for load in loads:
         load.start()
-    me = sp * 4 + tp
     barrier = pltpu.get_barrier_semaphore()
-
-    def greet(k, carry):
-        other = (me + k) % 128
-        pl.semaphore_signal(
-            barrier, inc=1, device_id=(other // 4, other % 4), device_id_type=MESH
-        )
-        return carry
-
-    lax.fori_loop(1, 128, greet, 0)
+    peers = [neighbour(d, k) for d in (0, 1) for k in (1, 3)] + [partner]
+    peers += [(sp, tp_at[k]) for k in (1, 2, 3)]
+    for peer in peers:
+        pl.semaphore_signal(barrier, inc=1, device_id=peer, device_id_type=MESH)
 
     turned = qa_ref[...].astype(F32).T.astype(BF16)
     nothing = jnp.zeros((64, rows), BF16)
@@ -137,7 +139,7 @@
     kv[sp, :, 128:384] = kb_ref[...]
     kv[sp, 0:128, 384:640] = va_ref[...].astype(F32).T.astype(BF16)
     kv[sp, 128:256, 384:640] = vb_ref[...].astype(F32).T.astype(BF16)
-    pl.semaphore_wait(barrier, 127)
+    pl.semaphore_wait(barrier, len(peers))
 
     started = []
 
@@ -145,7 +147,7 @@
         return (1, 0) if h == 0 else (0, 1)
 
     def piece_of(h, o1, o2):
-        return at(z - o2, y - o1, core) if h == 0 else at(z - o1, y - o2, core)
+        return at(-o2, -o1, 0) if h == 0 else at(-o1, -o2, 0)
 
     def half_send(h, o1, o2, along, step, part=None):
         dim = dims(h)[along]
@@ -189,7 +191,7 @@
         spread(h, o1, o2, 1)
 
     def pair_send(a, b):
-        p = at(z - a, y - b, core)
+        p = at(-a, -b, 0)
         copy = pltpu.make_async_remote_copy(
             src_ref=kv.at[p],
             dst_ref=kv.at[p],
@@ -250,10 +252,10 @@
             code += (a * 4 + b) * 16**k
 
         def body(k, left):
-            o = left % 16
+            o = lax.rem(left, 16)
             a = o // 4
-            b = o % 4
-            p = at(z - a, y - b, 1 - core)
+            b = lax.rem(o, 4)
+            p = lax.rem(z + 4 - a, 4) * 8 + lax.rem(y + 4 - b, 4) * 2 + 1 - core
             pltpu.make_async_copy(kv.at[p], kv.at[p], pair_sem.at[o]).wait()
             c = p // 2
 
@@ -269,7 +271,7 @@
         lane = lax.broadcasted_iota(jnp.int32, (64, 2048), 1)
         quarter = (lane // 4) % 4
         oz, oy, ox, oc = (table_ref[k : k + 1, :] for k in range(4))
-        expert = at(z + oz, y + oy, (core + oc) % 2) * 4 + (tp + ox) % 4
+        expert = (((z + oz) % 4) * 8 + ((y + oy) % 4) * 2 + (core + oc) % 2) * 4 + (tp + ox) % 4
         named = jnp.zeros((64, 2048), F32)
         mixed = jnp.zeros((64, 2048), F32)
         down = lax.broadcasted_iota(jnp.int32, (64, 64), 0)
@@ -362,7 +364,7 @@
         heads[:, :, head * 128 : head * 128 + 128] = done.astype(BF16).reshape(4, rows // 4, 128)
     sends = []
     for k in (1, 2, 3):
-        to = (tp + k) % 4
+        to = tp_at[k]
         copy = pltpu.make_async_remote_copy(
             src_ref=heads.at[to],
             dst_ref=back.at[tp],
@@ -377,7 +379,7 @@
     for load in loads:
         load.wait()
     for k in (1, 2, 3):
-        source = (tp + 4 - k) % 4
+        source = tp_at[4 - k]
         pltpu.make_async_copy(back.at[source], back.at[source], tp_recv.at[k]).wait()
 
     joined = jnp.concatenate(
@@ -385,20 +387,17 @@
     )
 
     def project(n, total):
-        cols = pl.ds(pl.multiple_of(n * 256, 256), 256)
+        cols = pl.ds(pl.multiple_of(n * 512, 512), 512)
         part = jnp.dot(joined, wo[:, cols], preferred_element_type=F32)
         rounded = (resid_ref[:, cols].astype(F32) + part).astype(BF16)
         middle[:, cols] = rounded
         wide = rounded.astype(F32)
         return total + jnp.sum(wide * wide, axis=1, keepdims=True)
 
-    total = lax.fori_loop(0, 8, project, jnp.zeros((64, 1), F32))
+    total = lax.fori_loop(0, 4, project, jnp.zeros((64, 1), F32), unroll=True)
     scale = lax.rsqrt(total / 2048.0 + EPSILON)
     normed = (middle[...].astype(F32) * scale * norm_ref[...]).astype(BF16)
     stack = jnp.concatenate([normed[:, j * 512 : j * 512 + 512] for j in range(4)], axis=0)
-
-    def device(o, other):
-        return (at(z + o[0], y + o[1], (core + other) % 2), (tp + o[2]) % 4)
 
     def move(source, target, sem_out, sem_in, o, other):
         pltpu.make_async_remote_copy(
@@ -486,14 +485,15 @@
             )
             rows_u = jnp.dot(perm[1], block, preferred_element_type=F32)
             res[s0 : s0 + 16] = rows_u.astype(BF16).reshape(16, 16, 512)
+            if u > 0:
+                direct(1, res, ret, s0 - 16, s0)
+        direct(1, res, ret, g * 64 + 48, g * 64 + 64 - g)
 
     arrived(0, recv, 0)
     expert(0)
-    direct(1, res, ret, 0, 64)
     arrived(0, recv, 1)
     expert(1)
     ret[127] = res[127]
-    direct(1, res, ret, 64, 127)
 
     for g in range(2):
         arrived(1, ret, g)

time: 113 us -> 107 us (0.947)
  Pallas kernels: 110 us -> 104 us
    pallas_call x1, Pallas kernels: 110 us -> 104 us  [layer(): pl.pallas_call(layer_kernel, out_shape=jax.ShapeDtypeStruct((tokens, widt...]
where the time goes in v6:
time: 107 us
  Pallas kernels  104 us (97%)
  local copies, waits for them, and re-layouts  1.67 us (2%)
  between operations  1.31 us (1%)
    pallas_call x1, Pallas kernels, layer(): pl.pallas_call(layer_kernel, out_shape=jax.ShapeDtypeStruct((tokens, widt...  104 us

profile of v6, /device:TPU:1, one launch (start us, length us, event | category | flops | bytes accessed | tf_op | source)
XLA Modules:
  0.0 106.7 jit_solution(12633558090727352553)
XLA Ops:
  1.3 103.7 %shard_map.199 = bf16[64,2048]{1,0:T(8,128)(2,1)} custom-call(bf16[256,128]{1,0:T(8,128)(2,1)} %bitcast.22, bf16[256,128]{1,0:T(8,128)(2,1)} %bitcast.23, bf16[256,128]{1,0:T(8,128)(2,1)} %bitcast.24, bf16[256,256]{1,0:T(8,128)(2,1)} %bitcast.20, bf16[256,256]{1,0:T(8,128)(2,1)} %bitcast.21, bf16[256,128]{1,0:T(8,128)(2,1)} %bitcast.25, ...), custom_call_target="tpu_custom_call" | custom-call | tf_op jit(solution)/shard_map/pallas_call | solution.py:531
  105.0 1.7 %copy.25 = bf16[64,2048]{1,0:T(8,128)(2,1)} copy(bf16[64,2048]{1,0:T(8,128)(2,1)} %shard_map.199) | data formatting | bytes 524288

commit v7 on v6

--- a/solution.py
+++ b/solution.py
@@ -30,6 +30,24 @@
 
 
 ORDER = flows()
+
+
+STEPS = (
+    ("a", [(1, 1, 0), (1, 3, 0), (0, 3, 0), (0, 0, 1), (0, 0, 3)]),
+    ("c", [(3, 0), (1, 0)]),
+    ("a", [(1, 0, 3), (0, 1, 0), (1, 0, 1), (0, 3, 3), (0, 0, 2), (1, 1, 3), (1, 1, 1), (0, 3, 1), (1, 2, 0)]),
+    ("c", [(0, 1), (0, 3)]),
+    ("a", [(0, 2, 0), (1, 3, 3)]),
+    ("c", [(2, 0)]),
+    ("a", [(0, 1, 3), (1, 0, 2), (0, 1, 1), (1, 3, 1)]),
+    ("c", [(1, 3), (3, 3), (0, 2), (1, 1)]),
+    ("a", [(1, 1, 2), (0, 2, 1), (1, 2, 1), (0, 3, 2), (1, 2, 3), (0, 2, 3)]),
+    ("c", [(3, 1)]),
+    ("a", [(1, 3, 2), (0, 1, 2)]),
+    ("c", [(1, 2), (2, 3)]),
+    ("a", [(1, 2, 2), (0, 2, 2)]),
+    ("c", [(2, 1), (3, 2), (2, 2)]),
+)
 
 
 def layer_kernel(
@@ -316,42 +334,17 @@
 
     slot_matrices()
 
-    for o1 in (1, 3):
-        for h in range(2):
-            arrive(h, o1, 0)
-    for o2 in (1, 3):
-        for h in range(2):
-            arrive(h, 0, o2)
-    near = [(0, 1), (0, 3), (1, 0), (3, 0)]
-    for a, b in near:
-        pair_send(a, b)
-    chunks(near)
-    for h in range(2):
-        arrive(h, 2, 0)
-    for o1 in (1, 3):
-        for o2 in (1, 3):
-            for h in range(2):
-                arrive(h, o1, o2)
-    for h in range(2):
-        arrive(h, 0, 2)
-    second = [(0, 2), (2, 0), (1, 1), (1, 3), (3, 1), (3, 3)]
-    for a, b in second:
-        pair_send(a, b)
-    chunks(second[:3])
-    for o2 in (1, 3):
-        for h in range(2):
-            arrive(h, 2, o2)
-    for o1 in (1, 3):
-        for h in range(2):
-            arrive(h, o1, 2)
-    third = [(1, 2), (3, 2), (2, 1), (2, 3)]
-    for a, b in third:
-        pair_send(a, b)
-    chunks(second[3:])
-    for h in range(2):
-        arrive(h, 2, 2)
-    pair_send(2, 2)
-    chunks(third + [(2, 2)])
+    whole = set()
+    for kind, items in STEPS:
+        if kind == "c":
+            chunks(items)
+            continue
+        for h, o1, o2 in items:
+            arrive(h, o1, o2)
+            whole.add((h, o1, o2))
+            a, b = (o2, o1) if h == 0 else (o1, o2)
+            if (0, b, a) in whole and (1, a, b) in whole:
+                pair_send(a, b)
 
     for head in range(2):
         first = acc[2 * head]

time: 107 us -> 105 us (0.981)
  Pallas kernels: 104 us -> 102 us
    pallas_call x1, Pallas kernels: 104 us -> 102 us  [layer(): pl.pallas_call(layer_kernel, out_shape=jax.ShapeDtypeStruct((tokens, widt...]
where the time goes in v7:
time: 105 us
  Pallas kernels  102 us (97%)
  local copies, waits for them, and re-layouts  1.67 us (2%)
  between operations  1.31 us (1%)
    pallas_call x1, Pallas kernels, layer(): pl.pallas_call(layer_kernel, out_shape=jax.ShapeDtypeStruct((tokens, widt...  102 us

profile of v7, /device:TPU:1, one launch (start us, length us, event | category | flops | bytes accessed | tf_op | source)
XLA Modules:
  0.0 104.9 jit_solution(8576542769612100042)
XLA Ops:
  1.3 102.0 %shard_map.199 = bf16[64,2048]{1,0:T(8,128)(2,1)} custom-call(bf16[256,128]{1,0:T(8,128)(2,1)} %bitcast.22, bf16[256,128]{1,0:T(8,128)(2,1)} %bitcast.23, bf16[256,128]{1,0:T(8,128)(2,1)} %bitcast.24, bf16[256,256]{1,0:T(8,128)(2,1)} %bitcast.20, bf16[256,256]{1,0:T(8,128)(2,1)} %bitcast.21, bf16[256,128]{1,0:T(8,128)(2,1)} %bitcast.25, ...), custom_call_target="tpu_custom_call" | custom-call | tf_op jit(solution)/shard_map/pallas_call | solution.py:524
  103.3 1.7 %copy.25 = bf16[64,2048]{1,0:T(8,128)(2,1)} copy(bf16[64,2048]{1,0:T(8,128)(2,1)} %shard_map.199) | data formatting | bytes 524288

commit v8 on v7

--- a/solution.py
+++ b/solution.py
@@ -25,7 +25,24 @@
     hops = np.minimum(mixed[:, :3], SIDE - mixed[:, :3]).sum(axis=1)
     mixed = mixed[np.argsort(-hops, kind="stable")]
     for part in (mixed[:64], mixed[64:]):
-        part[:] = part[np.random.RandomState(2).permutation(len(part))]
+        best = None
+        for seed in range(200):
+            trial = part[np.random.RandomState(seed).permutation(len(part))]
+            load = np.zeros((len(part), 7))
+            for k, o in enumerate(trial):
+                for d in range(3):
+                    v = o[d]
+                    if v == 2:
+                        load[k, 2 * d] += 1
+                        load[k, 2 * d + 1] += 1
+                    elif v:
+                        load[k, 2 * d + (v == 3)] += 1
+            run = np.cumsum(load[:, :6], axis=0)
+            ideal = np.arange(1, len(part) + 1)[:, None] * run[-1] / len(part)
+            score = np.abs(run - ideal).mean()
+            if best is None or score < best[0]:
+                best = (score, trial)
+        part[:] = best[1]
     return [tuple(int(v) for v in o) for o in mixed] + [(0, 0, 0, 0)]
 
 
@@ -463,14 +480,14 @@
             hs[:, cols] = (gate * jax.nn.sigmoid(gate) * up).astype(BF16)
             return carry
 
-        lax.fori_loop(0, 4, hidden, 0)
+        lax.fori_loop(0, 4, hidden, 0, unroll=2)
 
         def down(n, carry):
             cols = pl.ds(pl.multiple_of(n * 256, 256), 256)
             rs[:, cols] = jnp.dot(hs[...], wd[:, cols], preferred_element_type=F32).astype(BF16)
             return carry
 
-        lax.fori_loop(0, 8, down, 0)
+        lax.fori_loop(0, 8, down, 0, unroll=2)
         for u in range(4):
             s0 = (g * 4 + u) * 16
             block = jnp.concatenate(

time: 105 us -> 104 us (level)
  Pallas kernels: 102 us -> 100 us
    pallas_call x1, Pallas kernels: 102 us -> 100 us  [layer(): pl.pallas_call(layer_kernel, out_shape=jax.ShapeDtypeStruct((tokens, widt...]
where the time goes in v8:
time: 104 us; the launch traced here: 103 us
  Pallas kernels  100 us (96%)
  local copies, waits for them, and re-layouts  1.67 us (2%)
  between operations  1.31 us (1%)
    pallas_call x1, Pallas kernels, layer(): pl.pallas_call(layer_kernel, out_shape=jax.ShapeDtypeStruct((tokens, widt...  100 us

profile of v8, /device:TPU:1, one launch (start us, length us, event | category | flops | bytes accessed | tf_op | source)
XLA Modules:
  0.0 103.4 jit_solution(8040795274787334242)
XLA Ops:
  1.3 100.4 %shard_map.199 = bf16[64,2048]{1,0:T(8,128)(2,1)} custom-call(bf16[256,128]{1,0:T(8,128)(2,1)} %bitcast.22, bf16[256,128]{1,0:T(8,128)(2,1)} %bitcast.23, bf16[256,128]{1,0:T(8,128)(2,1)} %bitcast.24, bf16[256,256]{1,0:T(8,128)(2,1)} %bitcast.20, bf16[256,256]{1,0:T(8,128)(2,1)} %bitcast.21, bf16[256,128]{1,0:T(8,128)(2,1)} %bitcast.25, ...), custom_call_target="tpu_custom_call" | custom-call | tf_op jit(solution)/shard_map/pallas_call | solution.py:541
  101.7 1.7 %copy.25 = bf16[64,2048]{1,0:T(8,128)(2,1)} copy(bf16[64,2048]{1,0:T(8,128)(2,1)} %shard_map.199) | data formatting | bytes 524288

commit v9 on v8

--- a/solution.py
+++ b/solution.py
@@ -480,14 +480,14 @@
             hs[:, cols] = (gate * jax.nn.sigmoid(gate) * up).astype(BF16)
             return carry
 
-        lax.fori_loop(0, 4, hidden, 0, unroll=2)
+        lax.fori_loop(0, 4, hidden, 0, unroll=4)
 
         def down(n, carry):
             cols = pl.ds(pl.multiple_of(n * 256, 256), 256)
             rs[:, cols] = jnp.dot(hs[...], wd[:, cols], preferred_element_type=F32).astype(BF16)
             return carry
 
-        lax.fori_loop(0, 8, down, 0, unroll=2)
+        lax.fori_loop(0, 8, down, 0, unroll=4)
         for u in range(4):
             s0 = (g * 4 + u) * 16
             block = jnp.concatenate(

time: 104 us -> 103 us (level)
  no operation moved by 1% of the time
where the time goes in v9:
time: 103 us
  Pallas kernels  99.7 us (97%)
  local copies, waits for them, and re-layouts  1.67 us (2%)
  between operations  1.31 us (1%)
    pallas_call x1, Pallas kernels, layer(): pl.pallas_call(layer_kernel, out_shape=jax.ShapeDtypeStruct((tokens, widt...  99.7 us

profile of v9, /device:TPU:1, one launch (start us, length us, event | category | flops | bytes accessed | tf_op | source)
XLA Modules:
  0.0 102.7 jit_solution(14852773383471134554)
XLA Ops:
  1.3 99.7 %shard_map.199 = bf16[64,2048]{1,0:T(8,128)(2,1)} custom-call(bf16[256,128]{1,0:T(8,128)(2,1)} %bitcast.22, bf16[256,128]{1,0:T(8,128)(2,1)} %bitcast.23, bf16[256,128]{1,0:T(8,128)(2,1)} %bitcast.24, bf16[256,256]{1,0:T(8,128)(2,1)} %bitcast.20, bf16[256,256]{1,0:T(8,128)(2,1)} %bitcast.21, bf16[256,128]{1,0:T(8,128)(2,1)} %bitcast.25, ...), custom_call_target="tpu_custom_call" | custom-call | tf_op jit(solution)/shard_map/pallas_call | solution.py:541
  101.0 1.7 %copy.25 = bf16[64,2048]{1,0:T(8,128)(2,1)} copy(bf16[64,2048]{1,0:T(8,128)(2,1)} %shard_map.199) | data formatting | bytes 524288
